TPU v7x, 32 devices: a whole 2x2x4 slice. The times are simulated.
32 devices in a mesh: sp: 16 (over z, y, x), tp: 2 (over core).
Axes of the slice: x: 2, y: 2, z: 4, core: 2. Of those that a mesh axis runs over, the one named last changes fastest.
Arguments:
- residual: bfloat16 [3072, 2048], P(('sp', 'tp')), may hold values from -6 to 6
- queries: bfloat16 [3072, 1024], P('sp', 'tp'), may hold values from -6 to 6
- key_pairs: bfloat16 [3072, 1024], P('sp', 'tp'), may hold values from -6 to 6
- values: bfloat16 [3072, 1024], P('sp', 'tp'), may hold values from -6 to 6
- second_weight: float32 [8], P('tp'), may hold values from 0.3 to 0.8
- head_gain: float32 [1024], P('tp'), may hold values from 0.1 to 1.9
- out_weight: bfloat16 [1024, 2048], P('tp'), may hold values from -0.1875 to 0.1875
- norm_gain: float32 [2048], replicated, may hold values from 0.1 to 1.9
- up_weight: bfloat16 [2048, 5632], P('sp', 'tp'), may hold values from -0.125 to 0.125
- gate_weight: bfloat16 [2048, 5632], P('sp', 'tp'), may hold values from -0.125 to 0.125
- conv_weight: float32 [3, 5632], P(None, 'tp'), may hold values from -3.5 to 3.5
- conv_bias: float32 [5632], P('tp'), may hold values from -3 to 3
- down_weight: bfloat16 [5632, 2048], P('tp', 'sp'), may hold values from -0.078125 to 0.078125
Outputs:
- layer_out: bfloat16 [3072, 2048], P(('sp', 'tp'))
All inputs are finite; a program needn't handle non-finite values.
Results may differ from a plain program's by a relative error of at most 0.017.
Values may be sent and summed in bfloat16 or wider, within the bound.
A program may use at most 128 MiB of HBM per device.

v0:
```python
import functools
import math

import jax
import jax.numpy as jnp
from jax import lax
from jax.experimental import pallas as pl
from jax.experimental.pallas import tpu as pltpu
from jax.sharding import PartitionSpec as P

MESH = pl.DeviceIdType.MESH
VMEM_LIMIT = 60 * 1024 * 1024

HD = 64
VD = 128


eps = 1e-05
neg_fill = -1e30


def from_behind(value, axis, steps):
    count = lax.axis_size(axis)
    leading, last = (max(0, -steps), min(count, count - steps))
    return lax.ppermute(value, axis, [(source, source + steps) for source in range(leading, last)])


def normalize(rows_in, gain):
    values_f = rows_in.astype(jnp.float32)
    scale_inv = lax.rsqrt(jnp.mean(values_f * values_f, axis=-1, keepdims=True) + eps)
    return (values_f * scale_inv * gain).astype(jnp.bfloat16)


def attend(queries, key_pairs, values, second_weight, head_gain):
    tok_rows = queries.shape[0]
    head_count = second_weight.shape[0]
    sp_index = lax.axis_index("sp")
    query = queries.reshape(tok_rows, head_count, 2, HD)
    query_pos = sp_index * tok_rows + jnp.arange(tok_rows)
    last_query = (sp_index + 1) * tok_rows
    initial = (
        jnp.full((head_count, 2, tok_rows), neg_fill, jnp.float32),
        jnp.zeros((head_count, 2, tok_rows), jnp.float32),
        jnp.zeros((head_count, 2, tok_rows, VD), jnp.float32),
    )
    key_piece = lax.all_gather(key_pairs, "sp", axis=0, tiled=True)
    value_piece = lax.all_gather(values, "sp", axis=0, tiled=True)
    piece_len = key_piece.shape[0]

    def compute(state_in):
        maxima, totals, weighted = state_in
        key_rows = key_piece.reshape(piece_len, head_count, 2, HD)
        value_rows = value_piece.reshape(piece_len, head_count, VD)
        scores = jnp.einsum(
            "qhmd,khmd->hmqk", query, key_rows, preferred_element_type=jnp.float32
        ) * HD ** (-0.5)
        visible = jnp.arange(piece_len)[None, :] <= query_pos[:, None]
        scores = jnp.where(visible, scores, neg_fill)
        new_max = jnp.maximum(maxima, jnp.max(scores, axis=-1))
        exp_scores = jnp.where(visible, jnp.exp(scores - new_max[..., None]), jnp.float32(0.0))
        totals = jnp.sum(exp_scores, axis=-1)
        weighted = jnp.einsum(
            "hmqk,khe->hmqe",
            exp_scores.astype(jnp.bfloat16),
            value_rows,
            preferred_element_type=jnp.float32,
        )
        return (new_max, totals, weighted)

    def keep_state(state_in):
        return state_in

    maxima, totals, weighted = lax.cond(jnp.int32(0) < last_query, compute, keep_state, initial)
    diff = (
        weighted[:, 0] / totals[:, 0, :, None]
        - second_weight[:, None, None] * weighted[:, 1] / totals[:, 1, :, None]
    )
    diff = jnp.transpose(diff, (1, 0, 2))
    scale_inv = lax.rsqrt(jnp.mean(diff * diff, axis=-1, keepdims=True) + eps)
    attended = (
        (diff * scale_inv * head_gain.reshape(head_count, VD) * 0.8)
        .reshape(tok_rows, head_count * VD)
        .astype(jnp.bfloat16)
    )
    return attended


def local(
    residual,
    queries,
    key_pairs,
    values,
    second_weight,
    head_gain,
    out_weight,
    norm_gain,
    up_weight,
    gate_weight,
    conv_weight,
    conv_bias,
    down_weight,
):
    tok_rows = queries.shape[0]
    ff_local = up_weight.shape[1]
    attended = attend(queries, key_pairs, values, second_weight, head_gain)
    proj = lax.psum_scatter(
        jnp.dot(attended, out_weight, preferred_element_type=jnp.float32).astype(jnp.bfloat16),
        "tp",
        scatter_dimension=0,
        tiled=True,
    )
    mid = (residual.astype(jnp.float32) + proj.astype(jnp.float32)).astype(jnp.bfloat16)
    normed_all = lax.all_gather(normalize(mid, norm_gain), "tp", axis=0, tiled=True)
    up_sum = jnp.dot(
        normed_all,
        lax.all_gather(up_weight, "sp", axis=0, tiled=True),
        preferred_element_type=jnp.float32,
    )
    gate_sum = jnp.dot(
        normed_all,
        lax.all_gather(gate_weight, "sp", axis=0, tiled=True),
        preferred_element_type=jnp.float32,
    )
    up_proj = up_sum.astype(jnp.bfloat16)
    gate_proj = gate_sum.astype(jnp.bfloat16)
    taps = conv_weight.shape[0]
    rim_rows = from_behind(up_proj[tok_rows - (taps - 1) :], "sp", 1)
    extended = jnp.concatenate((rim_rows, up_proj), axis=0)
    conv_out = jnp.zeros((tok_rows, ff_local), jnp.float32) + conv_bias[None, :]
    for tap in range(taps):
        conv_out = conv_out + conv_weight[tap][None, :] * extended[tap : tap + tok_rows].astype(
            jnp.float32
        )
    hidden = (jax.nn.silu(conv_out) * gate_proj.astype(jnp.float32)).astype(jnp.bfloat16)
    down_all = lax.all_gather(down_weight, "sp", axis=1, tiled=True)
    ffn_out = lax.psum_scatter(
        jnp.dot(hidden, down_all, preferred_element_type=jnp.float32).astype(jnp.bfloat16),
        "tp",
        scatter_dimension=0,
        tiled=True,
    )
    return (mid.astype(jnp.float32) + ffn_out.astype(jnp.float32)).astype(jnp.bfloat16)


def greet(n, me, t):
    barrier = pltpu.get_barrier_semaphore()

    def signal(k, carry):
        pl.semaphore_signal(
            barrier, inc=1, device_id={"sp": lax.rem(me + k, n)}, device_id_type=MESH
        )
        return carry

    lax.fori_loop(1, n, signal, 0)
    pl.semaphore_signal(barrier, inc=1, device_id={"tp": 1 - t}, device_id_type=MESH)
    pl.semaphore_wait(barrier, n)


def to_sp(src, dst, send, recv, dest):
    return pltpu.make_async_remote_copy(
        src_ref=src, dst_ref=dst, send_sem=send, recv_sem=recv,
        device_id={"sp": dest}, device_id_type=MESH,
    )


def to_tp(src, dst, send, recv, dest):
    return pltpu.make_async_remote_copy(
        src_ref=src, dst_ref=dst, send_sem=send, recv_sem=recv,
        device_id={"tp": dest}, device_id_type=MESH,
    )


def gather_kernel(
    n, att, ow, res, gain, wu, wg, up, gate, mid,
    buf, pbuf, prbuf, psem, send, recv, fsend, frecv,
):
    me = lax.axis_index("sp")
    t = lax.axis_index("tp")
    half = res.shape[0]
    rows = 2 * half
    mine = pl.ds(pl.multiple_of(t * half, half), half)
    theirs = pl.ds(pl.multiple_of((1 - t) * half, half), half)
    greet(n, me, t)
    pbuf[...] = jnp.dot(att[theirs, :], ow[...], preferred_element_type=jnp.float32).astype(
        jnp.bfloat16
    )
    swap = to_tp(pbuf, prbuf, psem.at[0], psem.at[1], 1 - t)
    swap.start()
    own = jnp.dot(att[mine, :], ow[...], preferred_element_type=jnp.float32).astype(jnp.bfloat16)
    swap.wait()
    proj = (own.astype(jnp.float32) + prbuf[...].astype(jnp.float32)).astype(jnp.bfloat16)
    mid_v = (res[...].astype(jnp.float32) + proj.astype(jnp.float32)).astype(jnp.bfloat16)
    mid[...] = mid_v
    mid_f = mid_v.astype(jnp.float32)
    inv = lax.rsqrt(jnp.mean(mid_f * mid_f, axis=-1, keepdims=True) + eps)
    buf[0, mine, :] = (mid_f * inv * gain[...]).astype(jnp.bfloat16)

    p = plane_of(n)
    layers = n // p
    z, w = me // p, lax.rem(me, p)

    def column(a):
        dest = lax.rem(z + a, layers) * p + w
        return to_sp(buf.at[0, mine], buf.at[a * p, mine], send.at[a * p], recv.at[a * p], dest)

    def spread(a, b):
        slot = a * p + b
        dest = z * p + lax.rem(w + b, p)
        return to_sp(
            buf.at[a * p, mine], buf.at[slot, mine], send.at[slot], recv.at[slot], dest
        )

    def forward(k):
        return to_tp(buf.at[k, mine], buf.at[k, mine], fsend.at[k], frecv.at[k], 1 - t)

    def arrived(k):
        return to_tp(buf.at[k, theirs], buf.at[k, theirs], fsend.at[k], frecv.at[k], 1 - t)

    def relay(a):
        for b in range(1, p):
            spread(a, b).start()
        forward(a * p).start()

    def compute(a, b):
        arrived(a * p + b).wait_recv()
        source = lax.rem(z - a + layers, layers) * p + lax.rem(w - b + p, p)
        first = pl.multiple_of(source * rows, rows)
        block = buf[a * p + b]
        up[pl.ds(first, rows), :] = jnp.dot(
            block, wu[...], preferred_element_type=jnp.float32
        ).astype(jnp.bfloat16)
        gate[pl.ds(first, rows), :] = jnp.dot(
            block, wg[...], preferred_element_type=jnp.float32
        ).astype(jnp.bfloat16)

    for a in range(1, layers):
        column(a).start()
    relay(0)

    def stage(a, carry):
        @pl.when(a + 1 < layers)
        def _():
            column(a + 1).wait_recv()
            relay(a + 1)

        def step(b, carry):
            spread(a, b).wait_recv()
            forward(a * p + b).start()
            compute(a, b - 1)
            return carry

        lax.fori_loop(1, p, step, 0)
        compute(a, p - 1)
        return carry

    lax.fori_loop(0, layers, stage, 0)

    def drain(a, carry):
        for b in range(1, p):
            spread(a, b).wait_send()
            forward(a * p + b).wait_send()
        forward(a * p).wait_send()
        return carry

    lax.fori_loop(0, layers, drain, 0)
    for a in range(1, layers):
        column(a).wait_send()


def scatter_kernel(
    n, hid, down, mid, out, pb, pr, sb, rb, zb, cb, psend, precv, send, recv, zsend, zrecv,
):
    me = lax.axis_index("sp")
    t = lax.axis_index("tp")
    half = mid.shape[0]
    rows = 2 * half
    p = plane_of(n)
    layers = n // p
    z, w = me // p, lax.rem(me, p)
    greet(n, me, t)

    def place(i):
        return lax.rem(i // p + 1, layers), lax.rem(lax.rem(i, p) + 1, p)

    def swap(i):
        a, b = place(i)
        slot = a * p + b
        return to_tp(pb.at[slot], pr.at[slot], psend.at[slot], precv.at[slot], 1 - t)

    def across(a, b):
        slot = a * p + b
        dest = z * p + lax.rem(w + b, p)
        return to_sp(sb.at[slot], rb.at[slot], send.at[slot], recv.at[slot], dest)

    def column(a):
        dest = lax.rem(z + a, layers) * p + w
        return to_sp(zb.at[a], cb.at[a], zsend.at[a], zrecv.at[a], dest)

    def product(i):
        a, b = place(i)
        slot = a * p + b
        first = (lax.rem(z + a, layers) * p + lax.rem(w + b, p)) * rows
        theirs = pl.ds(pl.multiple_of(first + (1 - t) * half, half), half)
        mine = pl.ds(pl.multiple_of(first + t * half, half), half)
        pb[slot] = jnp.dot(hid[theirs, :], down[...], preferred_element_type=jnp.float32).astype(
            jnp.bfloat16
        )
        swap(i).start()
        sb[slot] = jnp.dot(hid[mine, :], down[...], preferred_element_type=jnp.float32).astype(
            jnp.bfloat16
        )

    def combine(i):
        a, b = place(i)
        slot = a * p + b
        swap(i).wait_recv()
        sb[slot] = (sb[slot].astype(jnp.float32) + pr[slot].astype(jnp.float32)).astype(
            jnp.bfloat16
        )

        @pl.when(b != 0)
        def _():
            across(a, b).start()

    def plane_sum(a):
        acc = sb[a * p].astype(jnp.float32)
        for b in range(1, p):
            across(a, b).wait_recv()
            acc = acc + rb[a * p + b].astype(jnp.float32)
        return acc

    product(0)

    def step(i, carry):
        product(i)
        combine(i - 1)

        @pl.when(jnp.logical_and(lax.rem(i, p) == p - 1, i >= p))
        def _():
            a = i // p
            zb[a] = plane_sum(a).astype(jnp.bfloat16)
            column(a).start()

        return carry

    lax.fori_loop(1, n, step, 0)
    combine(n - 1)
    acc = plane_sum(0)
    for a in range(1, layers):
        column(a).wait_recv()
        acc = acc + cb[a].astype(jnp.float32)
    ffn = acc.astype(jnp.bfloat16).astype(jnp.float32)
    out[...] = (mid[...].astype(jnp.float32) + ffn).astype(jnp.bfloat16)

    def drain(a, carry):
        for b in range(1, p):
            across(a, b).wait_send()
        for b in range(p):
            swap(a * p + b).wait_send()
        return carry

    lax.fori_loop(0, layers, drain, 0)
    for a in range(1, layers):
        column(a).wait_send()


def plane_of(n):
    return math.gcd(n, 4)


def vm(count):
    return [pl.BlockSpec(memory_space=pltpu.VMEM)] * count


def params(cid):
    return pltpu.CompilerParams(
        collective_id=cid, has_side_effects=True, vmem_limit_bytes=VMEM_LIMIT
    )


def gather_rows(n, att, ow, res, gain, wu, wg):
    half, width = res.shape
    units = wu.shape[1]
    rows = 2 * half
    bf = jnp.bfloat16
    dma = pltpu.SemaphoreType.DMA
    return pl.pallas_call(
        functools.partial(gather_kernel, n),
        out_shape=(
            jax.ShapeDtypeStruct((n * rows, units), bf),
            jax.ShapeDtypeStruct((n * rows, units), bf),
            jax.ShapeDtypeStruct((half, width), bf),
        ),
        in_specs=vm(6),
        out_specs=tuple(vm(3)),
        scratch_shapes=[
            pltpu.VMEM((n, rows, width), bf),
            pltpu.VMEM((half, width), bf),
            pltpu.VMEM((half, width), bf),
            dma((2,)), dma((n,)), dma((n,)), dma((n,)), dma((n,)),
        ],
        compiler_params=params(1),
        name="gather_rows",
    )(att, ow, res, gain[None, :], wu, wg)


def scatter_rows(n, hid, down, mid):
    half, width = mid.shape
    bf = jnp.bfloat16
    dma = pltpu.SemaphoreType.DMA
    layers = n // plane_of(n)
    block = pltpu.VMEM((n, half, width), bf)
    few = pltpu.VMEM((layers, half, width), bf)
    return pl.pallas_call(
        functools.partial(scatter_kernel, n),
        out_shape=jax.ShapeDtypeStruct((half, width), bf),
        in_specs=vm(3),
        out_specs=vm(1)[0],
        scratch_shapes=[block, block, block, block, few, few]
        + [dma((n,)), dma((n,)), dma((n,)), dma((n,)), dma((layers,)), dma((layers,))],
        compiler_params=params(2),
        name="scatter_rows",
    )(hid, down, mid)


def attention_kernel(
    n, heads, q, k, v, sw, gain, ub, gb, db, att, wu, wg, wd,
    qb, kb, vb, ob, qsend, qrecv, ksend, krecv, vsend, vrecv, osend, orecv,
    usend, urecv, gsend, grecv, dsend, drecv,
):
    me = lax.axis_index("sp")
    t = lax.axis_index("tp")
    rows = q.shape[0]
    depth = db.shape[2]
    groups = n // heads
    chunk = 2 * rows

    def cols(h):
        return pl.ds(pl.multiple_of(h * VD, VD), VD)

    def at(s):
        return pl.ds(pl.multiple_of(s * rows, rows), rows)

    def group_of(s):
        i, r = s // groups, lax.rem(s, groups)
        return jnp.where(lax.rem(i, 2) == 0, r, groups - 1 - r)

    head = lax.rem(me, heads)
    group = me // heads
    my_group = group_of(me)
    my_slot = me // groups
    greet(n, me, t)

    def query_copy(h):
        return to_sp(
            q.at[:, cols(h)], qb.at[my_slot], qsend.at[h], qrecv.at[my_slot], my_group * heads + h
        )

    def block_of(i):
        return i * groups + (group if i % 2 == 0 else groups - 1 - group)

    def query_wait(i):
        to_sp(qb.at[i], qb.at[i], qsend.at[0], qrecv.at[i], me).wait_recv()

    for h in range(heads):
        other = my_group * heads + h != me

        @pl.when(other)
        def _():
            query_copy(h).start()

        @pl.when(jnp.logical_not(other))
        def _():
            qb[my_slot] = q[:, cols(h)]

    def pair(d):
        dest = lax.rem(me + d, n)
        h = lax.rem(dest, heads)
        return (
            to_sp(k.at[:, cols(h)], kb.at[at(me)], ksend.at[d], krecv.at[d], dest),
            to_sp(v.at[:, cols(h)], vb.at[at(me)], vsend.at[d], vrecv.at[d], dest),
        )

    def weights(d):
        dest = lax.rem(me + d, n)
        wide = pl.ds(pl.multiple_of(me * depth, depth), depth)
        return (
            to_sp(ub.at[dest], wu.at[me], usend.at[d], urecv.at[d], dest),
            to_sp(gb.at[dest], wg.at[me], gsend.at[d], grecv.at[d], dest),
            to_sp(db.at[dest], wd.at[:, wide], dsend.at[d], drecv.at[d], dest),
        )

    def begin(make):
        def start(d, carry):
            for copy in make(d):
                copy.start()
            return carry

        lax.fori_loop(1, n, start, 0)

    def finish(make, sent):
        def wait(d, carry):
            for copy in make(d):
                if sent:
                    copy.wait_send()
                else:
                    copy.wait_recv()
            return carry

        lax.fori_loop(1, n, wait, 0)

    begin(pair)
    begin(weights)
    kb[at(me), :] = k[:, cols(head)]
    vb[at(me), :] = v[:, cols(head)]
    wu[me] = ub[me]
    wg[me] = gb[me]
    wd[:, pl.ds(pl.multiple_of(me * depth, depth), depth)] = db[me]
    for i in range(heads):

        @pl.when(block_of(i) != me)
        def _():
            query_wait(i)

    finish(pair, False)
    weight = sw[head]
    gain_row = gain[pl.ds(head, 1), :]
    lane = lax.broadcasted_iota(jnp.int32, (rows, VD), 1)

    def answer(i):
        return to_sp(
            ob.at[i], att.at[:, cols(head)], osend.at[i], orecv.at[head], block_of(i)
        )

    for i in range(heads):
        block = block_of(i)
        query = (qb[i].astype(jnp.float32) * HD ** (-0.5)).astype(jnp.bfloat16)
        zero = jnp.zeros_like(query)
        both = jnp.concatenate(
            (jnp.where(lane < HD, query, zero), jnp.where(lane < HD, zero, query)), axis=0
        )
        last = block // 2

        def visit(c, state, masked):
            top, total, acc = state
            span = pl.ds(pl.multiple_of(c * chunk, chunk), chunk)
            scores = lax.dot_general(
                both, kb[span, :], (((1,), (1,)), ((), ())), preferred_element_type=jnp.float32
            )
            if masked:
                row = lax.broadcasted_iota(jnp.int32, scores.shape, 0)
                row = jnp.where(row < rows, row, row - rows)
                col = lax.broadcasted_iota(jnp.int32, scores.shape, 1)
                visible = c * chunk + col <= block * rows + row
                scores = jnp.where(visible, scores, neg_fill)
            new_top = jnp.maximum(top, jnp.max(scores, axis=-1, keepdims=True))
            shrink = jnp.exp(top - new_top)
            exp_scores = jnp.exp(scores - new_top)
            total = total * shrink + jnp.sum(exp_scores, axis=-1, keepdims=True)
            acc = acc * shrink + jnp.dot(
                exp_scores.astype(jnp.bfloat16), vb[span, :], preferred_element_type=jnp.float32
            )
            return new_top, total, acc

        state = (
            jnp.full((2 * rows, 1), neg_fill, jnp.float32),
            jnp.zeros((2 * rows, 1), jnp.float32),
            jnp.zeros((2 * rows, VD), jnp.float32),
        )
        state = lax.fori_loop(0, last, lambda c, state: visit(c, state, False), state)
        top, total, acc = visit(last, state, True)
        mean_v = acc / total
        diff = mean_v[:rows] - weight * mean_v[rows:]
        inv = lax.rsqrt(jnp.mean(diff * diff, axis=-1, keepdims=True) + eps)
        result = (diff * inv * gain_row * 0.8).astype(jnp.bfloat16)

        @pl.when(block != me)
        def _():
            ob[i] = result
            answer(i).start()

        @pl.when(block == me)
        def _():
            att[:, cols(head)] = result

    for h in range(heads):
        other = my_group * heads + h != me

        @pl.when(other)
        def _():
            to_sp(ob.at[0], att.at[:, cols(h)], osend.at[0], orecv.at[h], me).wait_recv()
            query_copy(h).wait_send()

    for i in range(heads):

        @pl.when(block_of(i) != me)
        def _():
            answer(i).wait_send()

    finish(pair, True)
    finish(weights, False)
    finish(weights, True)


def attend_rows(n, q, k, v, second_weight, head_gain, up_weight, gate_weight, down_weight):
    rows, width = q.shape
    heads = second_weight.shape[0]
    depth, ff_local = up_weight.shape
    units = ff_local // n
    bf = jnp.bfloat16
    dma = pltpu.SemaphoreType.DMA
    ub = up_weight.reshape(depth, n, units).transpose(1, 0, 2)
    gb = gate_weight.reshape(depth, n, units).transpose(1, 0, 2)
    db = down_weight.reshape(n, units, depth)
    many = [dma((n,))]
    att, wu, wg, wd = pl.pallas_call(
        functools.partial(attention_kernel, n, heads),
        out_shape=(
            jax.ShapeDtypeStruct((rows, width), bf),
            jax.ShapeDtypeStruct((n, depth, units), bf),
            jax.ShapeDtypeStruct((n, depth, units), bf),
            jax.ShapeDtypeStruct((units, n * depth), bf),
        ),
        in_specs=vm(3) + [pl.BlockSpec(memory_space=pltpu.SMEM)] + vm(4),
        out_specs=tuple(vm(4)),
        scratch_shapes=[
            pltpu.VMEM((heads, rows, VD), bf),
            pltpu.VMEM((n * rows, VD), bf),
            pltpu.VMEM((n * rows, VD), bf),
            pltpu.VMEM((heads, rows, VD), bf),
            dma((heads,)), dma((heads,)),
        ]
        + many * 4
        + [dma((heads,)), dma((heads,))]
        + many * 6,
        compiler_params=params(0),
        name="attend_rows",
    )(q, k, v, second_weight, head_gain.reshape(heads, VD), ub, gb, db)
    return att, wu.reshape(n * depth, units), wg.reshape(n * depth, units), wd


def moving_rows(
    n,
    residual,
    queries,
    key_pairs,
    values,
    second_weight,
    head_gain,
    out_weight,
    norm_gain,
    up_weight,
    gate_weight,
    conv_weight,
    conv_bias,
    down_weight,
):
    sp_index = lax.axis_index("sp")
    units = up_weight.shape[1] // n
    taps = conv_weight.shape[0]
    cw = lax.dynamic_slice_in_dim(conv_weight, sp_index * units, units, 1)
    cb = lax.dynamic_slice_in_dim(conv_bias, sp_index * units, units, 0)
    attended, wu, wg, wd = attend_rows(
        n, queries, key_pairs, values, second_weight, head_gain, up_weight, gate_weight, down_weight
    )
    up, gate, mid = gather_rows(n, attended, out_weight, residual, norm_gain, wu, wg)
    count = up.shape[0]
    extended = jnp.pad(up, ((taps - 1, 0), (0, 0)))
    conv_out = jnp.zeros((count, units), jnp.float32) + cb[None, :]
    for tap in range(taps):
        conv_out = conv_out + cw[tap][None, :] * extended[tap : tap + count].astype(jnp.float32)
    hidden = (jax.nn.silu(conv_out) * gate.astype(jnp.float32)).astype(jnp.bfloat16)
    return scatter_rows(n, hidden, wd, mid)


def choose(n_sp, n_tp):
    def body(residual, queries, *rest):
        up_weight = rest[6]
        token_count = queries.shape[0] * n_sp
        width = residual.shape[1]
        moves_rows = (
            n_tp == 2
            and 2 * token_count < 3 * n_tp * up_weight.shape[1]
            and up_weight.shape[1] % n_sp == 0
            and n_sp % rest[2].shape[0] == 0
        )
        if moves_rows:
            return moving_rows(n_sp, residual, queries, *rest)
        return local(residual, queries, *rest)

    return body


def solution(mesh):
    return jax.shard_map(
        choose(mesh.shape["sp"], mesh.shape["tp"]),
        mesh=mesh,
        in_specs=(
            P(("sp", "tp"), None),
            P("sp", "tp"),
            P("sp", "tp"),
            P("sp", "tp"),
            P("tp"),
            P("tp"),
            P("tp", None),
            P(),
            P("sp", "tp"),
            P("sp", "tp"),
            P(None, "tp"),
            P("tp"),
            P("tp", "sp"),
        ),
        out_specs=P(("sp", "tp"), None),
        check_vma=False,
    )
```

profile of v0, /device:TPU:10, one launch (start us, length us, event | category | flops | bytes accessed | tf_op | source)
XLA Modules:
  0.0 294.8 jit_solution(8084387243583243667)
XLA Ops:
  0.0 0.0 copy-start
  0.0 1.5 copy.14
  1.5 1.3 copy.15
  2.8 0.0 copy-done
  2.8 0.3 copy.16
  3.2 1.3 copy.17
  4.5 120.6 %attend_rows.1 = (bf16[192,512]{1,0:T(8,128)(2,1)}, bf16[16,128,176]{2,1,0:T(8,128)(2,1)}, bf16[16,128,176]{2,1,0:T(8,128)(2,1)}, bf16[176,2048]{1,0:T(8,128)(2,1)}) custom-call(bf16[192,512]{1,0:T(8,128)(2,1)} %q.1, bf16[192,512]{1,0:T(8,128)(2,1)} %k.1, bf16[192,512]{1,0:T(8,128)(2,1)} %v.1, f32[4]{0:T(128)} %sw.1, f32[4,128]{1,0:T(4,128)} %bitcast.23, ...), custom_call_target="tpu_custom_call" | custom-call | tf_op jit(solution)/shard_map/attend_rows/pallas_call | solution.py:616
  125.1 80.3 %gather_rows.1 = (bf16[3072,176]{1,0:T(8,128)(2,1)}, bf16[3072,176]{1,0:T(8,128)(2,1)}, bf16[96,2048]{1,0:T(8,128)(2,1)}) custom-call(bf16[192,512]{1,0:T(8,128)(2,1)} %get-tuple-element.12.att, bf16[512,2048]{1,0:T(8,128)(2,1)} %ow.1, bf16[96,2048]{1,0:T(8,128)(2,1)} %res.1, f32[1,2048]{1,0:T(1,128)} %bitcast.19, bf16[2048,176]{1,0:T(8,128)(2,1)} %bitcast.16, ...), custom_call_target="tpu_custom_call" | custom-call | tf_op jit(solution)/shard_map/gather_rows/pallas_call | solution.py:387
  205.4 0.9 constant_dynamic-slice_fusion
  206.3 0.8 dynamic_slice.6
  207.0 5.4 %multiply_convert_fusion.hid = bf16[3072,176]{1,0:T(8,128)(2,1)} fusion(bf16[3072,176]{1,0:T(8,128)(2,1)} %get-tuple-element.16, bf16[3072,176]{1,0:T(8,128)(2,1)} %get-tuple-element.15, f32[176]{0:T(256)S(1)} %bitcast.22, f32[176]{0:T(256)S(1)} %bitcast.21, f32[176]{0:T(256)S(1)} %bitcast.20, f32[176]{0:T(256)S(1)} %dynamic_slice.6), kind=kLoop, calls=%fused_computation | loop fusion | flops 8650752 | bytes 3246848 | tf_op jit(solution)/shard_map/convert_element_type | solution.py:672
  212.4 80.6 %scatter_rows.1 = bf16[96,2048]{1,0:T(8,128)(2,1)} custom-call(bf16[3072,176]{1,0:T(8,128)(2,1)} %multiply_convert_fusion.hid, bf16[176,2048]{1,0:T(8,128)(2,1)} %get-tuple-element.17.down, bf16[96,2048]{1,0:T(8,128)(2,1)} %get-tuple-element.18.mid), custom_call_target="tpu_custom_call" | custom-call | tf_op jit(solution)/shard_map/scatter_rows/pallas_call | solution.py:414
  293.0 1.8 copy.19
Async XLA Ops:
  0.0 2.8 copy-start
where the time goes:
time: 298 us; the launch traced here: 295 us
  Pallas kernels  281 us (94%)
  local copies, waits for them, and re-layouts  7.88 us (3%)
  other arithmetic  5.37 us (2%)
    pallas_call x1, Pallas kernels, attend_rows(): pl.pallas_call(functools.partial(attention_kernel, n, heads), out_shape=(...  121 us
    pallas_call x1, Pallas kernels, scatter_rows(): pl.pallas_call(functools.partial(scatter_kernel, n), out_shape=jax.ShapeD...  80.6 us
    pallas_call x1, Pallas kernels, gather_rows(): pl.pallas_call(functools.partial(gather_kernel, n), out_shape=(jax.ShapeD...  80.3 us

commit v1 on v0

v1 whole, which is shorter than its diff:
```python
import functools

import jax
import jax.numpy as jnp
from jax import lax
from jax.experimental import pallas as pl
from jax.experimental.pallas import tpu as pltpu
from jax.sharding import PartitionSpec as P

MESH = pl.DeviceIdType.MESH
VMEM_LIMIT = 60 * 1024 * 1024

HD = 64
VD = 128


eps = 1e-05
neg_fill = -1e30


def from_behind(value, axis, steps):
    count = lax.axis_size(axis)
    leading, last = (max(0, -steps), min(count, count - steps))
    return lax.ppermute(value, axis, [(source, source + steps) for source in range(leading, last)])


def normalize(rows_in, gain):
    values_f = rows_in.astype(jnp.float32)
    scale_inv = lax.rsqrt(jnp.mean(values_f * values_f, axis=-1, keepdims=True) + eps)
    return (values_f * scale_inv * gain).astype(jnp.bfloat16)


def attend(queries, key_pairs, values, second_weight, head_gain):
    tok_rows = queries.shape[0]
    head_count = second_weight.shape[0]
    sp_index = lax.axis_index("sp")
    query = queries.reshape(tok_rows, head_count, 2, HD)
    query_pos = sp_index * tok_rows + jnp.arange(tok_rows)
    last_query = (sp_index + 1) * tok_rows
    initial = (
        jnp.full((head_count, 2, tok_rows), neg_fill, jnp.float32),
        jnp.zeros((head_count, 2, tok_rows), jnp.float32),
        jnp.zeros((head_count, 2, tok_rows, VD), jnp.float32),
    )
    key_piece = lax.all_gather(key_pairs, "sp", axis=0, tiled=True)
    value_piece = lax.all_gather(values, "sp", axis=0, tiled=True)
    piece_len = key_piece.shape[0]

    def compute(state_in):
        maxima, totals, weighted = state_in
        key_rows = key_piece.reshape(piece_len, head_count, 2, HD)
        value_rows = value_piece.reshape(piece_len, head_count, VD)
        scores = jnp.einsum(
            "qhmd,khmd->hmqk", query, key_rows, preferred_element_type=jnp.float32
        ) * HD ** (-0.5)
        visible = jnp.arange(piece_len)[None, :] <= query_pos[:, None]
        scores = jnp.where(visible, scores, neg_fill)
        new_max = jnp.maximum(maxima, jnp.max(scores, axis=-1))
        exp_scores = jnp.where(visible, jnp.exp(scores - new_max[..., None]), jnp.float32(0.0))
        totals = jnp.sum(exp_scores, axis=-1)
        weighted = jnp.einsum(
            "hmqk,khe->hmqe",
            exp_scores.astype(jnp.bfloat16),
            value_rows,
            preferred_element_type=jnp.float32,
        )
        return (new_max, totals, weighted)

    def keep_state(state_in):
        return state_in

    maxima, totals, weighted = lax.cond(jnp.int32(0) < last_query, compute, keep_state, initial)
    diff = (
        weighted[:, 0] / totals[:, 0, :, None]
        - second_weight[:, None, None] * weighted[:, 1] / totals[:, 1, :, None]
    )
    diff = jnp.transpose(diff, (1, 0, 2))
    scale_inv = lax.rsqrt(jnp.mean(diff * diff, axis=-1, keepdims=True) + eps)
    attended = (
        (diff * scale_inv * head_gain.reshape(head_count, VD) * 0.8)
        .reshape(tok_rows, head_count * VD)
        .astype(jnp.bfloat16)
    )
    return attended


def local(
    residual,
    queries,
    key_pairs,
    values,
    second_weight,
    head_gain,
    out_weight,
    norm_gain,
    up_weight,
    gate_weight,
    conv_weight,
    conv_bias,
    down_weight,
):
    tok_rows = queries.shape[0]
    ff_local = up_weight.shape[1]
    attended = attend(queries, key_pairs, values, second_weight, head_gain)
    proj = lax.psum_scatter(
        jnp.dot(attended, out_weight, preferred_element_type=jnp.float32).astype(jnp.bfloat16),
        "tp",
        scatter_dimension=0,
        tiled=True,
    )
    mid = (residual.astype(jnp.float32) + proj.astype(jnp.float32)).astype(jnp.bfloat16)
    normed_all = lax.all_gather(normalize(mid, norm_gain), "tp", axis=0, tiled=True)
    up_sum = jnp.dot(
        normed_all,
        lax.all_gather(up_weight, "sp", axis=0, tiled=True),
        preferred_element_type=jnp.float32,
    )
    gate_sum = jnp.dot(
        normed_all,
        lax.all_gather(gate_weight, "sp", axis=0, tiled=True),
        preferred_element_type=jnp.float32,
    )
    up_proj = up_sum.astype(jnp.bfloat16)
    gate_proj = gate_sum.astype(jnp.bfloat16)
    taps = conv_weight.shape[0]
    rim_rows = from_behind(up_proj[tok_rows - (taps - 1) :], "sp", 1)
    extended = jnp.concatenate((rim_rows, up_proj), axis=0)
    conv_out = jnp.zeros((tok_rows, ff_local), jnp.float32) + conv_bias[None, :]
    for tap in range(taps):
        conv_out = conv_out + conv_weight[tap][None, :] * extended[tap : tap + tok_rows].astype(
            jnp.float32
        )
    hidden = (jax.nn.silu(conv_out) * gate_proj.astype(jnp.float32)).astype(jnp.bfloat16)
    down_all = lax.all_gather(down_weight, "sp", axis=1, tiled=True)
    ffn_out = lax.psum_scatter(
        jnp.dot(hidden, down_all, preferred_element_type=jnp.float32).astype(jnp.bfloat16),
        "tp",
        scatter_dimension=0,
        tiled=True,
    )
    return (mid.astype(jnp.float32) + ffn_out.astype(jnp.float32)).astype(jnp.bfloat16)


def greet(n, me, t):
    barrier = pltpu.get_barrier_semaphore()

    def signal(k, carry):
        pl.semaphore_signal(
            barrier, inc=1, device_id={"sp": lax.rem(me + k, n)}, device_id_type=MESH
        )
        return carry

    lax.fori_loop(1, n, signal, 0)
    pl.semaphore_signal(barrier, inc=1, device_id={"tp": 1 - t}, device_id_type=MESH)
    pl.semaphore_wait(barrier, n)


def to_sp(src, dst, send, recv, dest):
    return pltpu.make_async_remote_copy(
        src_ref=src, dst_ref=dst, send_sem=send, recv_sem=recv,
        device_id={"sp": dest}, device_id_type=MESH,
    )


def to_tp(src, dst, send, recv, dest):
    return pltpu.make_async_remote_copy(
        src_ref=src, dst_ref=dst, send_sem=send, recv_sem=recv,
        device_id={"tp": dest}, device_id_type=MESH,
    )


def span(index, size):
    return pl.ds(pl.multiple_of(index * size, size), size)


def first_tile(group, tiles, groups):
    return group * tiles // groups


def tile_count(tiles, groups):
    return -(-tiles // groups)


class Place:
    def __init__(self, n):
        self.n = n
        self.layers = n // 4
        self.me = lax.axis_index("sp")
        self.t = lax.axis_index("tp")
        self.z = self.me // 4
        self.w = lax.rem(self.me, 4)
        self.y = self.w // 2
        self.x = lax.rem(self.w, 2)
        self.xn = self.z * 4 + self.y * 2 + (1 - self.x)
        self.yn = self.z * 4 + (1 - self.y) * 2 + self.x

    def ahead(self, a):
        return lax.rem(self.z + a, self.layers)

    def behind(self, a):
        return lax.rem(self.z - a + self.layers, self.layers)

    def chip(self, z, y, x):
        return z * 4 + y * 2 + x


def attention_kernel(
    n, q, k, v, sw, gain, ow, res, ngain, uw, gw, dw,
    mid, normed, wu, wg, wd,
    qb, kb, vb, ob, sb, att, pbuf, prbuf,
    zsend, zrecv, psend, precv, osend, orecv, tsem, wsend, wrecv, fsend, frecv,
):
    here = Place(n)
    me, t, z, w, y, x = here.me, here.t, here.z, here.w, here.y, here.x
    layers = here.layers
    rows = q.shape[0]
    half = rows // 2
    depth = uw.shape[0]
    groups = n // 2
    tiles = uw.shape[1] // VD
    wide = wu.shape[1]
    chunk = 4 * rows
    greet(n, me, t)

    def cols(h):
        return span(h, VD)

    def along_z(a):
        zz = here.ahead(a)
        dest = here.chip(zz, y, x)
        return (
            to_sp(k.at[:, cols(zz)], kb.at[span(me, rows)], zsend.at[0, a], zrecv.at[0, a], dest),
            to_sp(v.at[:, cols(zz)], vb.at[span(me, rows)], zsend.at[1, a], zrecv.at[1, a], dest),
            to_sp(q.at[:, cols(zz)], qb.at[z], zsend.at[2, a], zrecv.at[2, a], dest),
        )

    def in_plane(a):
        own = span(here.behind(a) * 4 + w, rows)
        return (
            to_sp(kb.at[own], kb.at[own], psend.at[0, a], precv.at[0, a], here.xn),
            to_sp(vb.at[own], vb.at[own], psend.at[1, a], precv.at[1, a], here.yn),
            to_sp(vb.at[own], vb.at[own], psend.at[2, a], precv.at[2, a], here.xn),
            to_sp(kb.at[own], kb.at[own], psend.at[3, a], precv.at[3, a], here.yn),
        )

    def corner(a):
        from_x = span(here.chip(here.behind(a), y, 1 - x), rows)
        from_y = span(here.chip(here.behind(a), 1 - y, x), rows)
        return (
            to_sp(kb.at[from_x], kb.at[from_x], psend.at[4, a], precv.at[4, a], here.yn),
            to_sp(vb.at[from_y], vb.at[from_y], psend.at[5, a], precv.at[5, a], here.xn),
        )

    def weights(a, b):
        slot = a * 2 + b
        zz = here.ahead(a)
        yy = lax.rem(y + b, 2)
        dest = here.chip(zz, yy, x)
        first = pl.multiple_of(first_tile(zz * 2 + yy, tiles, groups) * VD, VD)
        part = pl.ds(first, wide)
        mine = span(me, depth)
        return (
            to_sp(uw.at[:, part], wu.at[mine], wsend.at[0, slot], wrecv.at[0, slot], dest),
            to_sp(gw.at[:, part], wg.at[mine], wsend.at[1, slot], wrecv.at[1, slot], dest),
            to_sp(dw.at[part], wd.at[:, mine], wsend.at[2, slot], wrecv.at[2, slot], dest),
        )

    def across_x(a, b):
        slot = a * 2 + b
        got = span(here.chip(here.behind(a), lax.rem(y + b, 2), x), depth)
        return (
            to_sp(wu.at[got], wu.at[got], fsend.at[0, slot], frecv.at[0, slot], here.xn),
            to_sp(wg.at[got], wg.at[got], fsend.at[1, slot], frecv.at[1, slot], here.xn),
            to_sp(
                wd.at[:, got], wd.at[:, got], fsend.at[2, slot], frecv.at[2, slot], here.xn
            ),
        )

    def pass_on(a, b):
        for copy in weights(a, b):
            copy.wait_recv()
        for copy in across_x(a, b):
            copy.start()

    for a in range(1, layers):
        for copy in along_z(a):
            copy.start()
    kb[span(me, rows), :] = k[:, cols(z)]
    vb[span(me, rows), :] = v[:, cols(z)]
    qb[z] = q[:, cols(z)]
    for copy in in_plane(0):
        copy.start()
    for a in range(1, layers):
        for copy in weights(a, 0):
            copy.start()
    for copy in weights(0, 1):
        copy.start()
    own_first = pl.multiple_of(first_tile(z * 2 + y, tiles, groups) * VD, VD)
    own_part = pl.ds(own_first, wide)
    wu[span(me, depth), :] = uw[:, own_part]
    wg[span(me, depth), :] = gw[:, own_part]
    wd[:, span(me, depth)] = dw[own_part, :]

    def corner_stage(a):
        in_plane(a)[0].wait_recv()
        corner(a)[0].start()
        in_plane(a)[1].wait_recv()
        corner(a)[1].start()

    def stage(a, carry):
        copies = along_z(a)
        copies[0].wait_recv()
        copies[1].wait_recv()
        for copy in in_plane(a):
            copy.start()
        corner_stage(a - 1)
        return carry

    lax.fori_loop(1, layers, stage, 0)
    corner_stage(layers - 1)
    for copy in across_x(0, 0):
        copy.start()

    def settle(a, carry):
        in_plane(a)[2].wait_recv()
        in_plane(a)[3].wait_recv()
        corner(a)[0].wait_recv()
        corner(a)[1].wait_recv()
        return carry

    lax.fori_loop(0, layers, settle, 0)
    for a in range(1, layers):
        along_z(a)[2].wait_recv()

    weight = sw[z]
    gain_row = gain[pl.ds(z, 1), :]
    lane = lax.broadcasted_iota(jnp.int32, (rows, VD), 1)

    def answer(i):
        return to_sp(
            ob.at[i], att.at[:, cols(z)], osend.at[i], orecv.at[z], here.chip(i, y, x)
        )

    def fold(op, value):
        total = value[:, :VD]
        for j in range(1, chunk // VD):
            total = op(total, value[:, j * VD : (j + 1) * VD])
        return total

    def block(i, carry):
        query = (qb[i].astype(jnp.float32) * HD ** (-0.5)).astype(jnp.bfloat16)
        zero = jnp.zeros_like(query)
        both = jnp.concatenate(
            (jnp.where(lane < HD, query, zero), jnp.where(lane < HD, zero, query)), axis=0
        )

        def scores_of(c):
            return lax.dot_general(
                both, kb[span(c, chunk), :], (((1,), (1,)), ((), ())),
                preferred_element_type=jnp.float32,
            )

        def score(c, peak):
            scores = scores_of(c)
            sb[c] = scores
            return jnp.maximum(peak, fold(jnp.maximum, scores))

        peak = lax.fori_loop(0, i, score, jnp.full((2 * rows, VD), neg_fill, jnp.float32))
        scores = scores_of(i)
        row = lax.broadcasted_iota(jnp.int32, scores.shape, 0)
        row = jnp.where(row < rows, row, row - rows)
        col = lax.broadcasted_iota(jnp.int32, scores.shape, 1)
        scores = jnp.where(col <= w * rows + row, scores, neg_fill)
        sb[i] = scores
        peak = jnp.maximum(peak, fold(jnp.maximum, scores))
        top = jnp.max(peak, axis=-1, keepdims=True)

        def weigh(c, state):
            total, acc = state
            exp_scores = jnp.exp(sb[c] - top)
            total = total + fold(jnp.add, exp_scores)
            acc = acc + jnp.dot(
                exp_scores.astype(jnp.bfloat16), vb[span(c, chunk), :],
                preferred_element_type=jnp.float32,
            )
            return total, acc

        blank = jnp.zeros((2 * rows, VD), jnp.float32)
        total, acc = lax.fori_loop(0, i + 1, weigh, (blank, blank))
        mean_v = acc / jnp.sum(total, axis=-1, keepdims=True)
        diff = mean_v[:rows] - weight * mean_v[rows:]
        inv = lax.rsqrt(jnp.mean(diff * diff, axis=-1, keepdims=True) + eps)
        result = (diff * inv * gain_row * 0.8).astype(jnp.bfloat16)

        @pl.when(i != z)
        def _():
            ob[i] = result
            answer(i).start()

        @pl.when(i == z)
        def _():
            att[:, cols(z)] = result

        @pl.when(i == 0)
        def _():
            pass_on(0, 1)

        @pl.when(i > 0)
        def _():
            pass_on(jnp.maximum(i, 1), 0)

        return carry

    lax.fori_loop(0, layers, block, 0)
    for a in range(1, layers):
        for copy in weights(a, 1):
            copy.start()

    def answered(a, carry):
        h = here.behind(a)
        to_sp(ob.at[0], att.at[:, cols(h)], osend.at[0], orecv.at[h], me).wait_recv()
        return carry

    lax.fori_loop(1, layers, answered, 0)
    mine = span(t, half)
    theirs = span(1 - t, half)
    pbuf[...] = jnp.dot(att[theirs, :], ow[...], preferred_element_type=jnp.float32).astype(
        jnp.bfloat16
    )
    swap = to_tp(pbuf, prbuf, tsem.at[0], tsem.at[1], 1 - t)
    swap.start()
    own = jnp.dot(att[mine, :], ow[...], preferred_element_type=jnp.float32).astype(jnp.bfloat16)
    swap.wait()
    proj = (own.astype(jnp.float32) + prbuf[...].astype(jnp.float32)).astype(jnp.bfloat16)
    mid_v = (res[...].astype(jnp.float32) + proj.astype(jnp.float32)).astype(jnp.bfloat16)
    mid[...] = mid_v
    mid_f = mid_v.astype(jnp.float32)
    inv = lax.rsqrt(jnp.mean(mid_f * mid_f, axis=-1, keepdims=True) + eps)
    normed[...] = (mid_f * inv * ngain[...]).astype(jnp.bfloat16)

    def late(a, carry):
        pass_on(a, 1)
        return carry

    lax.fori_loop(1, layers, late, 0)

    def drain(a, carry):
        for b in range(2):
            for copy in across_x(a, b):
                copy.wait_recv()
                copy.wait_send()
        for copy in in_plane(a) + corner(a):
            copy.wait_send()

        @pl.when(a != z)
        def _():
            answer(a).wait_send()

        @pl.when(a > 0)
        def _():
            for copy in along_z(a) + weights(a, 0):
                copy.wait_send()

        for copy in weights(a, 1):
            copy.wait_send()
        return carry

    lax.fori_loop(0, layers, drain, 0)


def ffn_kernel(
    n, normed, mid, wu, wg, wd, cw, cb, out,
    buf, up, gate, tails, halo, hid, pb, pr, sb, rb, zb, cbuf,
    send, recv, fsend, frecv, hsend, hrecv,
    xsend, xrecv, ysend, yrecv, zsend, zrecv,
):
    here = Place(n)
    me, t, z, y, x = here.me, here.t, here.z, here.y, here.x
    layers = here.layers
    groups = n // 2
    half = mid.shape[0]
    rows = 2 * half
    rim = tails.shape[1]
    taps = cw.shape[0]
    wide = wu.shape[1]
    tiles = cw.shape[1] // VD
    mine = span(t, half)
    theirs = span(1 - t, half)
    greet(n, me, t)
    buf[0, mine, :] = normed[...]
    halo[0] = jnp.zeros(halo.shape[1:], jnp.bfloat16)

    def column(a):
        dest = here.chip(here.ahead(a), y, x)
        return to_sp(buf.at[0, mine], buf.at[a * 2, mine], send.at[a * 2], recv.at[a * 2], dest)

    def spread(a):
        return to_sp(
            buf.at[a * 2, mine], buf.at[a * 2 + 1, mine],
            send.at[a * 2 + 1], recv.at[a * 2 + 1], here.yn,
        )

    def forward(slot):
        return to_tp(
            buf.at[slot, mine], buf.at[slot, mine], fsend.at[slot], frecv.at[slot], 1 - t
        )

    def arrived(slot):
        return to_tp(
            buf.at[slot, theirs], buf.at[slot, theirs], fsend.at[slot], frecv.at[slot], 1 - t
        )

    def tail(j):
        return to_sp(tails.at[j], halo.at[j + 1], hsend.at[j], hrecv.at[j], here.xn)

    def compute(a, b):
        slot = a * 2 + b
        arrived(slot).wait_recv()
        j = here.behind(a) * 2 + lax.rem(y + b, 2)
        rows_in = buf[slot]
        up_v = jnp.dot(rows_in, wu[...], preferred_element_type=jnp.float32).astype(jnp.bfloat16)
        up[span(j, rows), :] = up_v
        tails[j] = up_v[rows - rim :]
        tail(j).start()
        gate[span(j, rows), :] = jnp.dot(
            rows_in, wg[...], preferred_element_type=jnp.float32
        ).astype(jnp.bfloat16)

    for a in range(1, layers):
        column(a).start()
    spread(0).start()
    forward(0).start()

    def stage(a, carry):
        @pl.when(a + 1 < layers)
        def _():
            column(a + 1).wait_recv()
            spread(a + 1).start()
            forward(2 * (a + 1)).start()

        compute(a, 0)
        spread(a).wait_recv()
        forward(2 * a + 1).start()
        compute(a, 1)
        return carry

    lax.fori_loop(0, layers, stage, 0)

    group = z * 2 + y
    start = first_tile(group, tiles, groups)
    before = first_tile(group - 1, tiles, groups) + wide // VD
    twice = jnp.where(group > 0, jnp.maximum(before - start, 0), 0) * VD
    part = pl.ds(pl.multiple_of(start * VD, VD), wide)

    def place(i):
        return lax.rem(i // 2 + 1, layers), lax.rem(lax.rem(i, 2) + 1, 2)

    def swap(slot):
        return to_tp(pb.at[slot], pr.at[slot], xsend.at[slot], xrecv.at[slot], 1 - t)

    def across(a):
        return to_sp(sb.at[a * 2 + 1], rb.at[a], ysend.at[a], yrecv.at[a], here.yn)

    def upright(a):
        dest = here.chip(here.ahead(a), y, x)
        return to_sp(zb.at[a], cbuf.at[a], zsend.at[a], zrecv.at[a], dest)

    def hidden(j):
        prior = jnp.where(x == 1, j, j - 1)

        @pl.when(prior >= 0)
        def _():
            tail(jnp.maximum(prior, 0)).wait_recv()

        edge = halo[prior + 1].astype(jnp.float32)
        now = up[span(j, rows), :].astype(jnp.float32)
        row = lax.broadcasted_iota(jnp.int32, now.shape, 0)
        conv = cb[:, part] + cw[pl.ds(taps - 1, 1), part] * now
        for back in range(1, taps):
            moved = pltpu.roll(now, back, 0)
            for r in range(back):
                moved = jnp.where(row == r, edge[rim - back + r][None, :], moved)
            conv = conv + cw[pl.ds(taps - 1 - back, 1), part] * moved
        act = conv / (1.0 + jnp.exp(-conv)) * gate[span(j, rows), :].astype(jnp.float32)
        lane = lax.broadcasted_iota(jnp.int32, act.shape, 1)
        hid[...] = jnp.where(lane < twice, 0.0, act).astype(jnp.bfloat16)

    def product(i):
        a, b = place(i)
        slot = a * 2 + b
        hidden(here.ahead(a) * 2 + lax.rem(y + b, 2))
        pb[slot] = jnp.dot(hid[theirs, :], wd[...], preferred_element_type=jnp.float32).astype(
            jnp.bfloat16
        )
        swap(slot).start()
        sb[slot] = jnp.dot(hid[mine, :], wd[...], preferred_element_type=jnp.float32).astype(
            jnp.bfloat16
        )

    def combine(i):
        a, b = place(i)
        slot = a * 2 + b
        swap(slot).wait_recv()
        sb[slot] = (sb[slot].astype(jnp.float32) + pr[slot].astype(jnp.float32)).astype(
            jnp.bfloat16
        )

        @pl.when(b != 0)
        def _():
            across(a).start()

    def plane_sum(a):
        across(a).wait_recv()
        return sb[a * 2].astype(jnp.float32) + rb[a].astype(jnp.float32)

    product(0)

    def step(i, carry):
        product(i)
        combine(i - 1)

        @pl.when(jnp.logical_and(lax.rem(i, 2) == 1, i >= 2))
        def _():
            a = i // 2
            zb[a] = plane_sum(a).astype(jnp.bfloat16)
            upright(a).start()

        return carry

    lax.fori_loop(1, groups, step, 0)
    combine(groups - 1)
    acc = plane_sum(0)
    for a in range(1, layers):
        upright(a).wait_recv()
        acc = acc + cbuf[a].astype(jnp.float32)
    ffn = acc.astype(jnp.bfloat16).astype(jnp.float32)
    out[...] = (mid[...].astype(jnp.float32) + ffn).astype(jnp.bfloat16)

    @pl.when(x == 0)
    def _():
        tail(groups - 1).wait_recv()

    def drain(a, carry):
        spread(a).wait_send()
        across(a).wait_send()
        for b in range(2):
            forward(a * 2 + b).wait_send()
            swap(a * 2 + b).wait_send()
            tail(a * 2 + b).wait_send()

        @pl.when(a > 0)
        def _():
            column(a).wait_send()
            upright(a).wait_send()

        return carry

    lax.fori_loop(0, layers, drain, 0)


def vm(count):
    return [pl.BlockSpec(memory_space=pltpu.VMEM)] * count


def params(cid):
    return pltpu.CompilerParams(
        collective_id=cid, has_side_effects=True, vmem_limit_bytes=VMEM_LIMIT
    )


def moving_rows(
    n,
    residual,
    queries,
    key_pairs,
    values,
    second_weight,
    head_gain,
    out_weight,
    norm_gain,
    up_weight,
    gate_weight,
    conv_weight,
    conv_bias,
    down_weight,
):
    rows, width = queries.shape
    half, model = residual.shape
    heads = second_weight.shape[0]
    depth, ff_local = up_weight.shape
    layers = n // 4
    groups = n // 2
    wide = tile_count(ff_local // VD, groups) * VD
    bf = jnp.bfloat16
    f32 = jnp.float32
    dma = pltpu.SemaphoreType.DMA
    shape = jax.ShapeDtypeStruct
    tall = shape((n * depth, wide), bf)
    mid, normed, wu, wg, wd = pl.pallas_call(
        functools.partial(attention_kernel, n),
        out_shape=(
            shape((half, model), bf), shape((half, model), bf),
            tall, tall, shape((wide, n * depth), bf),
        ),
        in_specs=vm(3) + [pl.BlockSpec(memory_space=pltpu.SMEM)] + vm(7),
        out_specs=tuple(vm(5)),
        scratch_shapes=[
            pltpu.VMEM((layers, rows, VD), bf),
            pltpu.VMEM((n * rows, VD), bf),
            pltpu.VMEM((n * rows, VD), bf),
            pltpu.VMEM((layers, rows, VD), bf),
            pltpu.VMEM((layers, 2 * rows, 4 * rows), f32),
            pltpu.VMEM((rows, width), bf),
            pltpu.VMEM((half, model), bf),
            pltpu.VMEM((half, model), bf),
            dma((3, layers)), dma((3, layers)),
            dma((6, layers)), dma((6, layers)),
            dma((layers,)), dma((layers,)), dma((2,)),
            dma((3, groups)), dma((3, groups)), dma((3, groups)), dma((3, groups)),
        ],
        compiler_params=params(0),
        name="attend_rows",
    )(
        queries, key_pairs, values, second_weight, head_gain.reshape(heads, VD),
        out_weight, residual, norm_gain[None, :], up_weight, gate_weight, down_weight,
    )
    block = pltpu.VMEM((groups, half, model), bf)
    few = pltpu.VMEM((layers, half, model), bf)
    rim = 16
    return pl.pallas_call(
        functools.partial(ffn_kernel, n),
        out_shape=shape((half, model), bf),
        in_specs=vm(7),
        out_specs=vm(1)[0],
        scratch_shapes=[
            pltpu.VMEM((groups, rows, model), bf),
            pltpu.VMEM((groups * rows, wide), bf),
            pltpu.VMEM((groups * rows, wide), bf),
            pltpu.VMEM((groups, rim, wide), bf),
            pltpu.VMEM((groups + 1, rim, wide), bf),
            pltpu.VMEM((rows, wide), bf),
            block, block, block, few, few, few,
        ]
        + [dma((groups,))] * 8
        + [dma((layers,))] * 4,
        compiler_params=params(1),
        name="ffn_rows",
    )(normed, mid, wu, wg, wd, conv_weight, conv_bias[None, :])


def choose(n_sp, n_tp):
    def body(residual, queries, *rest):
        up_weight = rest[6]
        moves_rows = (
            n_tp == 2
            and n_sp % 4 == 0
            and rest[2].shape[0] == n_sp // 4
            and up_weight.shape[1] % VD == 0
            and up_weight.shape[1] // VD >= n_sp // 2
            and queries.shape[0] % 32 == 0
            and up_weight.shape[0] % VD == 0
            and rest[8].shape[0] <= 16
        )
        if moves_rows:
            return moving_rows(n_sp, residual, queries, *rest)
        return local(residual, queries, *rest)

    return body


def solution(mesh):
    return jax.shard_map(
        choose(mesh.shape["sp"], mesh.shape["tp"]),
        mesh=mesh,
        in_specs=(
            P(("sp", "tp"), None),
            P("sp", "tp"),
            P("sp", "tp"),
            P("sp", "tp"),
            P("tp"),
            P("tp"),
            P("tp", None),
            P(),
            P("sp", "tp"),
            P("sp", "tp"),
            P(None, "tp"),
            P("tp"),
            P("tp", "sp"),
        ),
        out_specs=P(("sp", "tp"), None),
        check_vma=False,
    )
```

time: 298 us -> 207 us (0.69)
  Pallas kernels: 281 us -> 203 us
  other arithmetic: 5.37 us -> 0 us
  local copies, waits for them, and re-layouts: 7.88 us -> 3.08 us
    pallas_call x3 -> x2, Pallas kernels: 281 us -> 203 us  [the longest x1 111 us: moving_rows(): pl.pallas_call(functools.partial(ffn_kernel, n), out_shape=shape((half, m...]
    convert_element_type x1 -> x0, other arithmetic: 5.37 us -> none  [moving_rows(): (jax.nn.silu(conv_out) * gate.astype(jnp.float32)).astype(jnp.bfloat16)]
where the time goes in v1:
time: 207 us; the launch traced here: 206 us
  Pallas kernels  203 us (98%)
  local copies, waits for them, and re-layouts  3.08 us (1%)
    pallas_call x1, Pallas kernels, moving_rows(): pl.pallas_call(functools.partial(ffn_kernel, n), out_shape=shape((half, m...  111 us
    pallas_call x1, Pallas kernels, moving_rows(): pl.pallas_call(functools.partial(attention_kernel, n), out_shape=(shape((...  92.6 us

profile of v1, /device:TPU:10, one launch (start us, length us, event | category | flops | bytes accessed | tf_op | source)
XLA Modules:
  0.0 206.3 jit_solution(1916282540276470161)
XLA Ops:
  0.0 1.3 broadcast_in_dim.7.cb
  1.3 92.6 %attend_rows.1 = (bf16[96,2048]{1,0:T(8,128)(2,1)}, bf16[96,2048]{1,0:T(8,128)(2,1)}, bf16[2048,384]{1,0:T(8,128)(2,1)}, bf16[2048,384]{1,0:T(8,128)(2,1)}, bf16[384,2048]{1,0:T(8,128)(2,1)}) custom-call(bf16[192,512]{1,0:T(8,128)(2,1)} %q.1, bf16[192,512]{1,0:T(8,128)(2,1)} %k.1, bf16[192,512]{1,0:T(8,128)(2,1)} %v.1, f32[4]{0:T(128)} %sw.1, ...), custom_call_target="tpu_custom_call" | custom-call | tf_op jit(solution)/shard_map/attend_rows/pallas_call | solution.py:699
  93.9 110.7 %ffn_rows.1 = bf16[96,2048]{1,0:T(8,128)(2,1)} custom-call(bf16[96,2048]{1,0:T(8,128)(2,1)} %get-tuple-element.10.normed, bf16[96,2048]{1,0:T(8,128)(2,1)} %get-tuple-element.11.mid, bf16[2048,384]{1,0:T(8,128)(2,1)} %get-tuple-element.12.wu, bf16[2048,384]{1,0:T(8,128)(2,1)} %get-tuple-element.13.wg, bf16[384,2048]{1,0:T(8,128)(2,1)} %get-tuple-element.14.wd, ...), custom_call_target="tpu_custom_call" | custom-call | tf_op jit(solution)/shard_map/ffn_rows/pallas_call | solution.py:730
  204.6 1.8 copy.15

commit v2 on v1

--- a/solution.py
+++ b/solution.py
@@ -204,11 +204,14 @@
         return z * 4 + y * 2 + x
 
 
-def attention_kernel(
-    n, q, k, v, sw, gain, ow, res, ngain, uw, gw, dw,
-    mid, normed, wu, wg, wd,
-    qb, kb, vb, ob, sb, att, pbuf, prbuf,
+def layer_kernel(
+    n, q, k, v, sw, gain, ow, res, ngain, uw, gw, dw, cw, cb,
+    out,
+    wu, wg, wd, mid, qb, kb, vb, ob, sb, att, pbuf, prbuf,
+    buf, up, gate, tails, halo, hid, pb, pr, kept, rb, zb, cbuf,
     zsend, zrecv, psend, precv, osend, orecv, tsem, wsend, wrecv, fsend, frecv,
+    usend, dsend, lrecv, rsend, rrecv, csend, crecv, hsend, hrecv,
+    xsend, xrecv, ysend, yrecv, ssend, srecv,
 ):
     here = Place(n)
     me, t, z, w, y, x = here.me, here.t, here.z, here.w, here.y, here.x
@@ -436,88 +439,51 @@
     mid[...] = mid_v
     mid_f = mid_v.astype(jnp.float32)
     inv = lax.rsqrt(jnp.mean(mid_f * mid_f, axis=-1, keepdims=True) + eps)
-    normed[...] = (mid_f * inv * ngain[...]).astype(jnp.bfloat16)
-
-    def late(a, carry):
-        pass_on(a, 1)
-        return carry
-
-    lax.fori_loop(1, layers, late, 0)
-
-    def drain(a, carry):
-        for b in range(2):
-            for copy in across_x(a, b):
-                copy.wait_recv()
-                copy.wait_send()
-        for copy in in_plane(a) + corner(a):
-            copy.wait_send()
-
-        @pl.when(a != z)
-        def _():
-            answer(a).wait_send()
-
-        @pl.when(a > 0)
-        def _():
-            for copy in along_z(a) + weights(a, 0):
-                copy.wait_send()
-
-        for copy in weights(a, 1):
-            copy.wait_send()
-        return carry
-
-    lax.fori_loop(0, layers, drain, 0)
-
-
-def ffn_kernel(
-    n, normed, mid, wu, wg, wd, cw, cb, out,
-    buf, up, gate, tails, halo, hid, pb, pr, sb, rb, zb, cbuf,
-    send, recv, fsend, frecv, hsend, hrecv,
-    xsend, xrecv, ysend, yrecv, zsend, zrecv,
-):
-    here = Place(n)
-    me, t, z, y, x = here.me, here.t, here.z, here.y, here.x
-    layers = here.layers
-    groups = n // 2
-    half = mid.shape[0]
-    rows = 2 * half
+    home = z * 2 + y
+    buf[home, mine, :] = (mid_f * inv * ngain[...]).astype(jnp.bfloat16)
+    halo[0] = jnp.zeros(halo.shape[1:], jnp.bfloat16)
+
     rim = tails.shape[1]
     taps = cw.shape[0]
-    wide = wu.shape[1]
-    tiles = cw.shape[1] // VD
-    mine = span(t, half)
-    theirs = span(1 - t, half)
-    greet(n, me, t)
-    buf[0, mine, :] = normed[...]
-    halo[0] = jnp.zeros(halo.shape[1:], jnp.bfloat16)
-
-    def column(a):
-        dest = here.chip(here.ahead(a), y, x)
-        return to_sp(buf.at[0, mine], buf.at[a * 2, mine], send.at[a * 2], recv.at[a * 2], dest)
-
-    def spread(a):
+
+    def line_up(zz):
+        slot = zz * 2 + y
+        dest = here.chip(jnp.minimum(z + 1, layers - 1), y, x)
+        return to_sp(buf.at[slot, mine], buf.at[slot, mine], usend.at[zz], lrecv.at[zz], dest)
+
+    def line_down(zz):
+        slot = zz * 2 + y
+        dest = here.chip(jnp.maximum(z - 1, 0), y, x)
+        return to_sp(buf.at[slot, mine], buf.at[slot, mine], dsend.at[zz], lrecv.at[zz], dest)
+
+    def spread(zz):
+        slot = zz * 2 + y
         return to_sp(
-            buf.at[a * 2, mine], buf.at[a * 2 + 1, mine],
-            send.at[a * 2 + 1], recv.at[a * 2 + 1], here.yn,
+            buf.at[slot, mine], buf.at[slot, mine], rsend.at[zz], rrecv.at[zz], here.yn
+        )
+
+    def spread_in(zz):
+        slot = zz * 2 + 1 - y
+        return to_sp(
+            buf.at[slot, mine], buf.at[slot, mine], rsend.at[zz], rrecv.at[zz], here.yn
         )
 
     def forward(slot):
         return to_tp(
-            buf.at[slot, mine], buf.at[slot, mine], fsend.at[slot], frecv.at[slot], 1 - t
+            buf.at[slot, mine], buf.at[slot, mine], csend.at[slot], crecv.at[slot], 1 - t
         )
 
     def arrived(slot):
         return to_tp(
-            buf.at[slot, theirs], buf.at[slot, theirs], fsend.at[slot], frecv.at[slot], 1 - t
+            buf.at[slot, theirs], buf.at[slot, theirs], csend.at[slot], crecv.at[slot], 1 - t
         )
 
     def tail(j):
         return to_sp(tails.at[j], halo.at[j + 1], hsend.at[j], hrecv.at[j], here.xn)
 
-    def compute(a, b):
-        slot = a * 2 + b
-        arrived(slot).wait_recv()
-        j = here.behind(a) * 2 + lax.rem(y + b, 2)
-        rows_in = buf[slot]
+    def compute(j):
+        arrived(j).wait_recv()
+        rows_in = buf[j]
         up_v = jnp.dot(rows_in, wu[...], preferred_element_type=jnp.float32).astype(jnp.bfloat16)
         up[span(j, rows), :] = up_v
         tails[j] = up_v[rows - rim :]
@@ -526,44 +492,118 @@
             rows_in, wg[...], preferred_element_type=jnp.float32
         ).astype(jnp.bfloat16)
 
-    for a in range(1, layers):
-        column(a).start()
-    spread(0).start()
-    forward(0).start()
-
-    def stage(a, carry):
-        @pl.when(a + 1 < layers)
-        def _():
-            column(a + 1).wait_recv()
-            spread(a + 1).start()
-            forward(2 * (a + 1)).start()
-
-        compute(a, 0)
-        spread(a).wait_recv()
-        forward(2 * a + 1).start()
-        compute(a, 1)
-        return carry
-
-    lax.fori_loop(0, layers, stage, 0)
-
-    group = z * 2 + y
-    start = first_tile(group, tiles, groups)
-    before = first_tile(group - 1, tiles, groups) + wide // VD
-    twice = jnp.where(group > 0, jnp.maximum(before - start, 0), 0) * VD
+    @pl.when(z + 1 < layers)
+    def _():
+        line_up(z).start()
+
+    @pl.when(z > 0)
+    def _():
+        line_down(z).start()
+
+    spread(z).start()
+    forward(home).start()
+
+    def late(a, carry):
+        pass_on(a, 1)
+        return carry
+
+    lax.fori_loop(1, layers, late, 0)
+
+    def line_step(d):
+        low, high = z - d, z + d
+
+        @pl.when(low >= 0)
+        def _():
+            line_up(low).wait_recv()
+
+            @pl.when(z + 1 < layers)
+            def _():
+                line_up(low).start()
+
+            spread(low).start()
+            forward(low * 2 + y).start()
+
+        @pl.when(high < layers)
+        def _():
+            line_down(high).wait_recv()
+
+            @pl.when(z > 0)
+            def _():
+                line_down(high).start()
+
+            spread(high).start()
+            forward(high * 2 + y).start()
+
+    line_step(1)
+
+    def crossed(a, carry):
+        for b in range(2):
+            for copy in across_x(a, b):
+                copy.wait_recv()
+        return carry
+
+    lax.fori_loop(0, layers, crossed, 0)
+
+    def stage_rows(d, carry):
+        @pl.when(jnp.logical_and(d > 0, d + 1 < layers))
+        def _():
+            line_step(d + 1)
+
+        low, high = z - d, z + d
+        has_low = low >= 0
+        has_high = jnp.logical_and(high < layers, d > 0)
+
+        @pl.when(has_low)
+        def _():
+            compute(low * 2 + y)
+            spread_in(low).wait_recv()
+            forward(low * 2 + 1 - y).start()
+
+        @pl.when(has_high)
+        def _():
+            compute(high * 2 + y)
+            spread_in(high).wait_recv()
+            forward(high * 2 + 1 - y).start()
+
+        @pl.when(has_low)
+        def _():
+            compute(low * 2 + 1 - y)
+
+        @pl.when(has_high)
+        def _():
+            compute(high * 2 + 1 - y)
+
+        return carry
+
+    lax.fori_loop(0, layers, stage_rows, 0)
+
+    start = first_tile(home, tiles, groups)
+    before = first_tile(home - 1, tiles, groups) + wide // VD
+    twice = jnp.where(home > 0, jnp.maximum(before - start, 0), 0) * VD
     part = pl.ds(pl.multiple_of(start * VD, VD), wide)
-
-    def place(i):
-        return lax.rem(i // 2 + 1, layers), lax.rem(lax.rem(i, 2) + 1, 2)
-
-    def swap(slot):
+    bias = jnp.concatenate([cb[pl.ds(start + j, 1), :] for j in range(wide // VD)], axis=1)
+
+    below, above = z, layers - 1 - z
+
+    def order(i):
+        lead = jnp.abs(above - below)
+        k = i - lead
+        more_above = above >= below
+        far = jnp.where(more_above, layers - 1 - i, i)
+        near_even = jnp.where(more_above, k // 2, layers - 1 - k // 2)
+        near_odd = jnp.where(more_above, layers - 1 - lead - k // 2, lead + k // 2)
+        near = jnp.where(lax.rem(k + layers * 2, 2) == 0, near_even, near_odd)
+        pick = jnp.where(i < lead, far, near)
+        return jnp.where(i >= layers - 1, z, pick)
+
+    def swap_sums(slot):
         return to_tp(pb.at[slot], pr.at[slot], xsend.at[slot], xrecv.at[slot], 1 - t)
 
-    def across(a):
-        return to_sp(sb.at[a * 2 + 1], rb.at[a], ysend.at[a], yrecv.at[a], here.yn)
-
-    def upright(a):
-        dest = here.chip(here.ahead(a), y, x)
-        return to_sp(zb.at[a], cbuf.at[a], zsend.at[a], zrecv.at[a], dest)
+    def across(zz):
+        return to_sp(kept.at[zz * 2 + 1 - y], rb.at[zz], ysend.at[zz], yrecv.at[zz], here.yn)
+
+    def chain(zz, landing, dest):
+        return to_sp(zb.at[zz], cbuf.at[landing], ssend.at[zz], srecv.at[landing], dest)
 
     def hidden(j):
         prior = jnp.where(x == 1, j, j - 1)
@@ -575,64 +615,91 @@
         edge = halo[prior + 1].astype(jnp.float32)
         now = up[span(j, rows), :].astype(jnp.float32)
         row = lax.broadcasted_iota(jnp.int32, now.shape, 0)
-        conv = cb[:, part] + cw[pl.ds(taps - 1, 1), part] * now
+        conv = bias + cw[pl.ds(taps - 1, 1), part] * now
         for back in range(1, taps):
             moved = pltpu.roll(now, back, 0)
             for r in range(back):
                 moved = jnp.where(row == r, edge[rim - back + r][None, :], moved)
             conv = conv + cw[pl.ds(taps - 1 - back, 1), part] * moved
         act = conv / (1.0 + jnp.exp(-conv)) * gate[span(j, rows), :].astype(jnp.float32)
-        lane = lax.broadcasted_iota(jnp.int32, act.shape, 1)
-        hid[...] = jnp.where(lane < twice, 0.0, act).astype(jnp.bfloat16)
+        lane_of = lax.broadcasted_iota(jnp.int32, act.shape, 1)
+        hid[...] = jnp.where(lane_of < twice, 0.0, act).astype(jnp.bfloat16)
+
+    def slot_of(i):
+        side = jnp.where(i < layers, 1 - y, y)
+        return order(lax.rem(i, layers)) * 2 + side
 
     def product(i):
-        a, b = place(i)
-        slot = a * 2 + b
-        hidden(here.ahead(a) * 2 + lax.rem(y + b, 2))
+        slot = slot_of(i)
+        hidden(slot)
         pb[slot] = jnp.dot(hid[theirs, :], wd[...], preferred_element_type=jnp.float32).astype(
             jnp.bfloat16
         )
-        swap(slot).start()
-        sb[slot] = jnp.dot(hid[mine, :], wd[...], preferred_element_type=jnp.float32).astype(
+        swap_sums(slot).start()
+        kept[slot] = jnp.dot(hid[mine, :], wd[...], preferred_element_type=jnp.float32).astype(
             jnp.bfloat16
         )
 
     def combine(i):
-        a, b = place(i)
-        slot = a * 2 + b
-        swap(slot).wait_recv()
-        sb[slot] = (sb[slot].astype(jnp.float32) + pr[slot].astype(jnp.float32)).astype(
+        slot = slot_of(i)
+        swap_sums(slot).wait_recv()
+        kept[slot] = (kept[slot].astype(jnp.float32) + pr[slot].astype(jnp.float32)).astype(
             jnp.bfloat16
         )
 
-        @pl.when(b != 0)
-        def _():
-            across(a).start()
-
-    def plane_sum(a):
-        across(a).wait_recv()
-        return sb[a * 2].astype(jnp.float32) + rb[a].astype(jnp.float32)
+        @pl.when(i < layers)
+        def _():
+            across(order(i)).start()
 
     product(0)
 
     def step(i, carry):
         product(i)
         combine(i - 1)
-
-        @pl.when(jnp.logical_and(lax.rem(i, 2) == 1, i >= 2))
-        def _():
-            a = i // 2
-            zb[a] = plane_sum(a).astype(jnp.bfloat16)
-            upright(a).start()
-
         return carry
 
     lax.fori_loop(1, groups, step, 0)
     combine(groups - 1)
-    acc = plane_sum(0)
-    for a in range(1, layers):
-        upright(a).wait_recv()
-        acc = acc + cbuf[a].astype(jnp.float32)
+
+    def row_sum(zz):
+        across(zz).wait_recv()
+        return kept[zz * 2 + y].astype(jnp.float32) + rb[zz].astype(jnp.float32)
+
+    def link(i, carry):
+        zz = order(i)
+        rising = zz > z
+        fed = jnp.where(rising, z > 0, z + 1 < layers)
+        total = row_sum(zz)
+
+        @pl.when(fed)
+        def _():
+            chain(zz, zz, me).wait_recv()
+            zb[zz] = (total + cbuf[zz].astype(jnp.float32)).astype(jnp.bfloat16)
+
+        @pl.when(jnp.logical_not(fed))
+        def _():
+            zb[zz] = total.astype(jnp.bfloat16)
+
+        nz = jnp.where(rising, z + 1, z - 1)
+        landing = jnp.where(jnp.logical_and(nz == zz, jnp.logical_not(rising)), layers, zz)
+        chain(zz, landing, here.chip(nz, y, x)).start()
+        return carry
+
+    lax.fori_loop(0, layers - 1, link, 0)
+    total = row_sum(z)
+    cbuf[layers + 1] = jnp.zeros(cbuf.shape[1:], jnp.bfloat16)
+
+    @pl.when(z > 0)
+    def _():
+        chain(z, z, me).wait_recv()
+
+    @pl.when(z + 1 < layers)
+    def _():
+        chain(z, layers, me).wait_recv()
+
+    from_low = cbuf[jnp.where(z > 0, z, layers + 1)].astype(jnp.float32)
+    from_high = cbuf[jnp.where(z + 1 < layers, layers, layers + 1)].astype(jnp.float32)
+    acc = total + from_low + from_high
     ffn = acc.astype(jnp.bfloat16).astype(jnp.float32)
     out[...] = (mid[...].astype(jnp.float32) + ffn).astype(jnp.bfloat16)
 
@@ -641,18 +708,37 @@
         tail(groups - 1).wait_recv()
 
     def drain(a, carry):
+        for b in range(2):
+            for copy in across_x(a, b):
+                copy.wait_send()
+            forward(a * 2 + b).wait_send()
+            swap_sums(a * 2 + b).wait_send()
+            tail(a * 2 + b).wait_send()
+        for copy in in_plane(a) + corner(a):
+            copy.wait_send()
         spread(a).wait_send()
         across(a).wait_send()
-        for b in range(2):
-            forward(a * 2 + b).wait_send()
-            swap(a * 2 + b).wait_send()
-            tail(a * 2 + b).wait_send()
+
+        @pl.when(a != z)
+        def _():
+            answer(a).wait_send()
+            chain(a, a, me).wait_send()
+
+        @pl.when(jnp.logical_and(a <= z, z + 1 < layers))
+        def _():
+            line_up(a).wait_send()
+
+        @pl.when(jnp.logical_and(a >= z, z > 0))
+        def _():
+            line_down(a).wait_send()
 
         @pl.when(a > 0)
         def _():
-            column(a).wait_send()
-            upright(a).wait_send()
-
+            for copy in along_z(a) + weights(a, 0):
+                copy.wait_send()
+
+        for copy in weights(a, 1):
+            copy.wait_send()
         return carry
 
     lax.fori_loop(0, layers, drain, 0)
@@ -660,12 +746,6 @@
 
 def vm(count):
     return [pl.BlockSpec(memory_space=pltpu.VMEM)] * count
-
-
-def params(cid):
-    return pltpu.CompilerParams(
-        collective_id=cid, has_side_effects=True, vmem_limit_bytes=VMEM_LIMIT
-    )
 
 
 def moving_rows(
@@ -690,62 +770,49 @@
     depth, ff_local = up_weight.shape
     layers = n // 4
     groups = n // 2
-    wide = tile_count(ff_local // VD, groups) * VD
+    tiles = ff_local // VD
+    wide = tile_count(tiles, groups) * VD
+    rim = 16
     bf = jnp.bfloat16
     f32 = jnp.float32
     dma = pltpu.SemaphoreType.DMA
-    shape = jax.ShapeDtypeStruct
-    tall = shape((n * depth, wide), bf)
-    mid, normed, wu, wg, wd = pl.pallas_call(
-        functools.partial(attention_kernel, n),
-        out_shape=(
-            shape((half, model), bf), shape((half, model), bf),
-            tall, tall, shape((wide, n * depth), bf),
-        ),
-        in_specs=vm(3) + [pl.BlockSpec(memory_space=pltpu.SMEM)] + vm(7),
-        out_specs=tuple(vm(5)),
+
+    def room(*dims):
+        return pltpu.VMEM(dims, bf)
+
+    return pl.pallas_call(
+        functools.partial(layer_kernel, n),
+        out_shape=jax.ShapeDtypeStruct((half, model), bf),
+        in_specs=vm(3) + [pl.BlockSpec(memory_space=pltpu.SMEM)] + vm(9),
+        out_specs=vm(1)[0],
         scratch_shapes=[
-            pltpu.VMEM((layers, rows, VD), bf),
-            pltpu.VMEM((n * rows, VD), bf),
-            pltpu.VMEM((n * rows, VD), bf),
-            pltpu.VMEM((layers, rows, VD), bf),
+            room(n * depth, wide), room(n * depth, wide), room(wide, n * depth),
+            room(half, model),
+            room(layers, rows, VD), room(n * rows, VD), room(n * rows, VD),
+            room(layers, rows, VD),
             pltpu.VMEM((layers, 2 * rows, 4 * rows), f32),
-            pltpu.VMEM((rows, width), bf),
-            pltpu.VMEM((half, model), bf),
-            pltpu.VMEM((half, model), bf),
-            dma((3, layers)), dma((3, layers)),
-            dma((6, layers)), dma((6, layers)),
+            room(rows, width), room(half, model), room(half, model),
+            room(groups, rows, model), room(groups * rows, wide), room(groups * rows, wide),
+            room(groups, rim, wide), room(groups + 1, rim, wide), room(rows, wide),
+            room(groups, half, model), room(groups, half, model), room(groups, half, model),
+            room(layers, half, model), room(layers, half, model), room(layers + 2, half, model),
+            dma((3, layers)), dma((3, layers)), dma((6, layers)), dma((6, layers)),
             dma((layers,)), dma((layers,)), dma((2,)),
             dma((3, groups)), dma((3, groups)), dma((3, groups)), dma((3, groups)),
+            dma((layers,)), dma((layers,)), dma((layers,)), dma((layers,)), dma((layers,)),
+            dma((groups,)), dma((groups,)), dma((groups,)), dma((groups,)),
+            dma((groups,)), dma((groups,)), dma((layers,)), dma((layers,)),
+            dma((layers,)), dma((layers + 1,)),
         ],
-        compiler_params=params(0),
-        name="attend_rows",
+        compiler_params=pltpu.CompilerParams(
+            collective_id=0, has_side_effects=True, vmem_limit_bytes=VMEM_LIMIT
+        ),
+        name="layer_rows",
     )(
         queries, key_pairs, values, second_weight, head_gain.reshape(heads, VD),
         out_weight, residual, norm_gain[None, :], up_weight, gate_weight, down_weight,
-    )
-    block = pltpu.VMEM((groups, half, model), bf)
-    few = pltpu.VMEM((layers, half, model), bf)
-    rim = 16
-    return pl.pallas_call(
-        functools.partial(ffn_kernel, n),
-        out_shape=shape((half, model), bf),
-        in_specs=vm(7),
-        out_specs=vm(1)[0],
-        scratch_shapes=[
-            pltpu.VMEM((groups, rows, model), bf),
-            pltpu.VMEM((groups * rows, wide), bf),
-            pltpu.VMEM((groups * rows, wide), bf),
-            pltpu.VMEM((groups, rim, wide), bf),
-            pltpu.VMEM((groups + 1, rim, wide), bf),
-            pltpu.VMEM((rows, wide), bf),
-            block, block, block, few, few, few,
-        ]
-        + [dma((groups,))] * 8
-        + [dma((layers,))] * 4,
-        compiler_params=params(1),
-        name="ffn_rows",
-    )(normed, mid, wu, wg, wd, conv_weight, conv_bias[None, :])
+        conv_weight, conv_bias.reshape(tiles, VD),
+    )
 
 
 def choose(n_sp, n_tp):

time: 207 us -> 164 us (0.79)
  Pallas kernels: 203 us -> 160 us
    pallas_call x2 -> x1, Pallas kernels: 203 us -> 160 us  [moving_rows(): pl.pallas_call(functools.partial(layer_kernel, n), out_shape=jax.ShapeDty...]
where the time goes in v2:
time: 164 us; the launch traced here: 162 us
  Pallas kernels  160 us (98%)
  local copies, waits for them, and re-layouts  1.77 us (1%)
    pallas_call x1, Pallas kernels, moving_rows(): pl.pallas_call(functools.partial(layer_kernel, n), out_shape=jax.ShapeDty...  160 us

profile of v2, /device:TPU:10, one launch (start us, length us, event | category | flops | bytes accessed | tf_op | source)
XLA Modules:
  0.0 161.6 jit_solution(5301288228253864624)
XLA Ops:
  0.0 159.8 %layer_rows.1 = bf16[96,2048]{1,0:T(8,128)(2,1)} custom-call(bf16[192,512]{1,0:T(8,128)(2,1)} %q.1, bf16[192,512]{1,0:T(8,128)(2,1)} %k.1, bf16[192,512]{1,0:T(8,128)(2,1)} %v.1, f32[4]{0:T(128)} %sw.1, f32[4,128]{1,0:T(4,128)} %bitcast.5, bf16[512,2048]{1,0:T(8,128)(2,1)} %ow.1, bf16[96,2048]{1,0:T(8,128)(2,1)} %res.1, f32[1,2048]{1,0:T(1,128)} %bitcast.4, ...), custom_call_target="tpu_custom_call" | custom-call | tf_op jit(solution)/shard_map/layer_rows/pallas_call | solution.py:783
  159.9 1.8 %copy.15 = bf16[96,2048]{1,0:T(8,128)(2,1)} copy(bf16[96,2048]{1,0:T(8,128)(2,1)} %layer_rows.1) | data formatting | bytes 786432

commit v3 on v2

--- a/solution.py
+++ b/solution.py
@@ -16,6 +16,7 @@
 
 eps = 1e-05
 neg_fill = -1e30
+PIECES = 4
 
 
 def from_behind(value, axis, steps):
@@ -207,9 +208,9 @@
 def layer_kernel(
     n, q, k, v, sw, gain, ow, res, ngain, uw, gw, dw, cw, cb,
     out,
-    wu, wg, wd, mid, qb, kb, vb, ob, sb, att, pbuf, prbuf,
+    wu, wg, wd, owb, resb, mid, qb, kb, vb, ob, sb, att, pbuf, prbuf,
     buf, up, gate, tails, halo, hid, pb, pr, kept, rb, zb, cbuf,
-    zsend, zrecv, psend, precv, osend, orecv, tsem, wsend, wrecv, fsend, frecv,
+    lsem, zsend, zrecv, psend, precv, osend, orecv, tsem, wsend, wrecv, fsend, frecv,
     usend, dsend, lrecv, rsend, rrecv, csend, crecv, hsend, hrecv,
     xsend, xrecv, ysend, yrecv, ssend, srecv,
 ):
@@ -223,7 +224,6 @@
     tiles = uw.shape[1] // VD
     wide = wu.shape[1]
     chunk = 4 * rows
-    greet(n, me, t)
 
     def cols(h):
         return span(h, VD)
@@ -254,36 +254,109 @@
             to_sp(vb.at[from_y], vb.at[from_y], psend.at[5, a], precv.at[5, a], here.xn),
         )
 
-    def weights(a, b):
+    most = wide - VD
+    cuts = (slice(0, most), slice(most, wide))
+
+    def begins(group):
+        return first_tile(group, tiles, groups)
+
+    def is_full(group):
+        return begins(group + 1) - begins(group) == wide // VD
+
+    own_group = z * 2 + y
+    full = is_full(own_group)
+
+    def target(a, b):
+        return here.ahead(a), lax.rem(y + b, 2)
+
+    def weights(a, b, cut):
         slot = a * 2 + b
-        zz = here.ahead(a)
-        yy = lax.rem(y + b, 2)
+        zz, yy = target(a, b)
         dest = here.chip(zz, yy, x)
-        first = pl.multiple_of(first_tile(zz * 2 + yy, tiles, groups) * VD, VD)
-        part = pl.ds(first, wide)
-        mine = span(me, depth)
+        first = pl.multiple_of(begins(zz * 2 + yy) * VD + cuts[cut].start, VD)
+        part = pl.ds(first, cuts[cut].stop - cuts[cut].start)
+        place = span(me, depth)
+        k = cut * 3
         return (
-            to_sp(uw.at[:, part], wu.at[mine], wsend.at[0, slot], wrecv.at[0, slot], dest),
-            to_sp(gw.at[:, part], wg.at[mine], wsend.at[1, slot], wrecv.at[1, slot], dest),
-            to_sp(dw.at[part], wd.at[:, mine], wsend.at[2, slot], wrecv.at[2, slot], dest),
-        )
-
-    def across_x(a, b):
+            to_sp(
+                uw.at[:, part], wu.at[place, cuts[cut]],
+                wsend.at[k, slot], wrecv.at[k, slot], dest,
+            ),
+            to_sp(
+                gw.at[:, part], wg.at[place, cuts[cut]],
+                wsend.at[k + 1, slot], wrecv.at[k + 1, slot], dest,
+            ),
+            to_sp(
+                dw.at[part], wd.at[cuts[cut], place],
+                wsend.at[k + 2, slot], wrecv.at[k + 2, slot], dest,
+            ),
+        )
+
+    def across_x(a, b, cut):
         slot = a * 2 + b
         got = span(here.chip(here.behind(a), lax.rem(y + b, 2), x), depth)
+        k = cut * 3
+        return tuple(
+            to_sp(ref, ref, fsend.at[k + i, slot], frecv.at[k + i, slot], here.xn)
+            for i, ref in enumerate(
+                (wu.at[got, cuts[cut]], wg.at[got, cuts[cut]], wd.at[cuts[cut], got])
+            )
+        )
+
+    def both_cuts(make, whole, act):
+        for copy in make(0):
+            act(copy)
+
+        @pl.when(whole)
+        def _():
+            for copy in make(1):
+                act(copy)
+
+    def whole_target(a, b):
+        zz, yy = target(a, b)
+        return is_full(zz * 2 + yy)
+
+    def send_weights(a, b):
+        both_cuts(lambda cut: weights(a, b, cut), whole_target(a, b), lambda c: c.start())
+
+    def sent_weights(a, b):
+        both_cuts(lambda cut: weights(a, b, cut), whole_target(a, b), lambda c: c.wait_send())
+
+    def send_across(a, b):
+        both_cuts(lambda cut: across_x(a, b, cut), full, lambda c: c.start())
+
+    def sent_across(a, b):
+        both_cuts(lambda cut: across_x(a, b, cut), full, lambda c: c.wait_send())
+
+    def got_across(a, b):
+        both_cuts(lambda cut: across_x(a, b, cut), full, lambda c: c.wait_recv())
+
+    def pass_on(a, b):
+        both_cuts(lambda cut: weights(a, b, cut), full, lambda c: c.wait_recv())
+        send_across(a, b)
+
+    def own_copies(cut):
+        first = pl.multiple_of(begins(own_group) * VD + cuts[cut].start, VD)
+        part = pl.ds(first, cuts[cut].stop - cuts[cut].start)
+        place = span(me, depth)
+        k = cut * 3
         return (
-            to_sp(wu.at[got], wu.at[got], fsend.at[0, slot], frecv.at[0, slot], here.xn),
-            to_sp(wg.at[got], wg.at[got], fsend.at[1, slot], frecv.at[1, slot], here.xn),
-            to_sp(
-                wd.at[:, got], wd.at[:, got], fsend.at[2, slot], frecv.at[2, slot], here.xn
-            ),
-        )
-
-    def pass_on(a, b):
-        for copy in weights(a, b):
-            copy.wait_recv()
-        for copy in across_x(a, b):
-            copy.start()
+            pltpu.make_async_copy(uw.at[:, part], wu.at[place, cuts[cut]], lsem.at[k]),
+            pltpu.make_async_copy(gw.at[:, part], wg.at[place, cuts[cut]], lsem.at[k + 1]),
+            pltpu.make_async_copy(dw.at[part], wd.at[cuts[cut], place], lsem.at[k + 2]),
+        )
+
+    def side_copies():
+        return (
+            pltpu.make_async_copy(ow, owb, lsem.at[6]),
+            pltpu.make_async_copy(res, resb, lsem.at[7]),
+        )
+
+    both_cuts(own_copies, full, lambda c: c.start())
+    for copy in side_copies():
+        copy.start()
+
+    greet(n, me, t)
 
     for a in range(1, layers):
         for copy in along_z(a):
@@ -294,15 +367,16 @@
     for copy in in_plane(0):
         copy.start()
     for a in range(1, layers):
-        for copy in weights(a, 0):
-            copy.start()
-    for copy in weights(0, 1):
-        copy.start()
-    own_first = pl.multiple_of(first_tile(z * 2 + y, tiles, groups) * VD, VD)
-    own_part = pl.ds(own_first, wide)
-    wu[span(me, depth), :] = uw[:, own_part]
-    wg[span(me, depth), :] = gw[:, own_part]
-    wd[:, span(me, depth)] = dw[own_part, :]
+        send_weights(a, 0)
+    send_weights(0, 1)
+
+    @pl.when(jnp.logical_not(full))
+    def _():
+        wu[:, cuts[1]] = jnp.zeros((wu.shape[0], VD), jnp.bfloat16)
+        wg[:, cuts[1]] = jnp.zeros((wu.shape[0], VD), jnp.bfloat16)
+        wd[cuts[1], :] = jnp.zeros((VD, wd.shape[1]), jnp.bfloat16)
+
+    both_cuts(own_copies, full, lambda c: c.wait())
 
     def corner_stage(a):
         in_plane(a)[0].wait_recv()
@@ -321,8 +395,7 @@
 
     lax.fori_loop(1, layers, stage, 0)
     corner_stage(layers - 1)
-    for copy in across_x(0, 0):
-        copy.start()
+    send_across(0, 0)
 
     def settle(a, carry):
         in_plane(a)[2].wait_recv()
@@ -416,8 +489,7 @@
 
     lax.fori_loop(0, layers, block, 0)
     for a in range(1, layers):
-        for copy in weights(a, 1):
-            copy.start()
+        send_weights(a, 1)
 
     def answered(a, carry):
         h = here.behind(a)
@@ -425,17 +497,19 @@
         return carry
 
     lax.fori_loop(1, layers, answered, 0)
+    for copy in side_copies():
+        copy.wait()
     mine = span(t, half)
     theirs = span(1 - t, half)
-    pbuf[...] = jnp.dot(att[theirs, :], ow[...], preferred_element_type=jnp.float32).astype(
+    pbuf[...] = jnp.dot(att[theirs, :], owb[...], preferred_element_type=jnp.float32).astype(
         jnp.bfloat16
     )
     swap = to_tp(pbuf, prbuf, tsem.at[0], tsem.at[1], 1 - t)
     swap.start()
-    own = jnp.dot(att[mine, :], ow[...], preferred_element_type=jnp.float32).astype(jnp.bfloat16)
+    own = jnp.dot(att[mine, :], owb[...], preferred_element_type=jnp.float32).astype(jnp.bfloat16)
     swap.wait()
     proj = (own.astype(jnp.float32) + prbuf[...].astype(jnp.float32)).astype(jnp.bfloat16)
-    mid_v = (res[...].astype(jnp.float32) + proj.astype(jnp.float32)).astype(jnp.bfloat16)
+    mid_v = (resb[...].astype(jnp.float32) + proj.astype(jnp.float32)).astype(jnp.bfloat16)
     mid[...] = mid_v
     mid_f = mid_v.astype(jnp.float32)
     inv = lax.rsqrt(jnp.mean(mid_f * mid_f, axis=-1, keepdims=True) + eps)
@@ -538,8 +612,7 @@
 
     def crossed(a, carry):
         for b in range(2):
-            for copy in across_x(a, b):
-                copy.wait_recv()
+            got_across(a, b)
         return carry
 
     lax.fori_loop(0, layers, crossed, 0)
@@ -548,6 +621,13 @@
         @pl.when(jnp.logical_and(d > 0, d + 1 < layers))
         def _():
             line_step(d + 1)
+
+        @pl.when(d == layers - 1)
+        def _():
+            product(layers - 2)
+            product(groups - 2)
+            combine(layers - 2)
+            combine(groups - 2)
 
         low, high = z - d, z + d
         has_low = low >= 0
@@ -575,11 +655,8 @@
 
         return carry
 
-    lax.fori_loop(0, layers, stage_rows, 0)
-
     start = first_tile(home, tiles, groups)
-    before = first_tile(home - 1, tiles, groups) + wide // VD
-    twice = jnp.where(home > 0, jnp.maximum(before - start, 0), 0) * VD
+    real = (begins(home + 1) - start) * VD
     part = pl.ds(pl.multiple_of(start * VD, VD), wide)
     bias = jnp.concatenate([cb[pl.ds(start + j, 1), :] for j in range(wide // VD)], axis=1)
 
@@ -599,11 +676,21 @@
     def swap_sums(slot):
         return to_tp(pb.at[slot], pr.at[slot], xsend.at[slot], xrecv.at[slot], 1 - t)
 
-    def across(zz):
-        return to_sp(kept.at[zz * 2 + 1 - y], rb.at[zz], ysend.at[zz], yrecv.at[zz], here.yn)
-
-    def chain(zz, landing, dest):
-        return to_sp(zb.at[zz], cbuf.at[landing], ssend.at[zz], srecv.at[landing], dest)
+    strip = out.shape[1] // PIECES
+    strips = [slice(h * strip, (h + 1) * strip) for h in range(PIECES)]
+
+    def across(zz, h):
+        s = zz * PIECES + h
+        return to_sp(
+            kept.at[zz * 2 + 1 - y, :, strips[h]], rb.at[zz, :, strips[h]],
+            ysend.at[s], yrecv.at[s], here.yn,
+        )
+
+    def chain(zz, landing, dest, h):
+        return to_sp(
+            zb.at[zz, :, strips[h]], cbuf.at[landing, :, strips[h]],
+            ssend.at[zz * PIECES + h], srecv.at[landing * PIECES + h], dest,
+        )
 
     def hidden(j):
         prior = jnp.where(x == 1, j, j - 1)
@@ -623,7 +710,7 @@
             conv = conv + cw[pl.ds(taps - 1 - back, 1), part] * moved
         act = conv / (1.0 + jnp.exp(-conv)) * gate[span(j, rows), :].astype(jnp.float32)
         lane_of = lax.broadcasted_iota(jnp.int32, act.shape, 1)
-        hid[...] = jnp.where(lane_of < twice, 0.0, act).astype(jnp.bfloat16)
+        hid[...] = jnp.where(lane_of < real, act, 0.0).astype(jnp.bfloat16)
 
     def slot_of(i):
         side = jnp.where(i < layers, 1 - y, y)
@@ -649,59 +736,83 @@
 
         @pl.when(i < layers)
         def _():
-            across(order(i)).start()
-
-    product(0)
-
-    def step(i, carry):
-        product(i)
-        combine(i - 1)
-        return carry
-
-    lax.fori_loop(1, groups, step, 0)
-    combine(groups - 1)
-
-    def row_sum(zz):
-        across(zz).wait_recv()
-        return kept[zz * 2 + y].astype(jnp.float32) + rb[zz].astype(jnp.float32)
-
-    def link(i, carry):
-        zz = order(i)
+            for h in range(PIECES):
+                across(order(i), h).start()
+
+    def row_sum(zz, h):
+        across(zz, h).wait_recv()
+        return kept[zz * 2 + y, :, strips[h]].astype(jnp.float32) + rb[zz, :, strips[h]].astype(
+            jnp.float32
+        )
+
+    def send_on(zz):
         rising = zz > z
         fed = jnp.where(rising, z > 0, z + 1 < layers)
-        total = row_sum(zz)
-
-        @pl.when(fed)
-        def _():
-            chain(zz, zz, me).wait_recv()
-            zb[zz] = (total + cbuf[zz].astype(jnp.float32)).astype(jnp.bfloat16)
-
-        @pl.when(jnp.logical_not(fed))
-        def _():
-            zb[zz] = total.astype(jnp.bfloat16)
-
         nz = jnp.where(rising, z + 1, z - 1)
         landing = jnp.where(jnp.logical_and(nz == zz, jnp.logical_not(rising)), layers, zz)
-        chain(zz, landing, here.chip(nz, y, x)).start()
+        for h in range(PIECES):
+            total = row_sum(zz, h)
+
+            @pl.when(fed)
+            def _():
+                chain(zz, zz, me, h).wait_recv()
+                zb[zz, :, strips[h]] = (
+                    total + cbuf[zz, :, strips[h]].astype(jnp.float32)
+                ).astype(jnp.bfloat16)
+
+            @pl.when(jnp.logical_not(fed))
+            def _():
+                zb[zz, :, strips[h]] = total.astype(jnp.bfloat16)
+
+            chain(zz, landing, here.chip(nz, y, x), h).start()
+
+    lax.fori_loop(0, layers, stage_rows, 0)
+    at_end = jnp.logical_or(z == 0, z == layers - 1)
+
+    @pl.when(at_end)
+    def _():
+        send_on(order(layers - 2))
+
+    def later(i):
+        skip = jnp.where(i < layers - 2, i, i + 1)
+        return jnp.where(skip < groups - 2, skip, skip + 1)
+
+    product(later(0))
+
+    def step(i, carry):
+        product(later(i))
+        combine(later(i - 1))
+        return carry
+
+    lax.fori_loop(1, groups - 2, step, 0)
+    combine(later(groups - 3))
+
+    cbuf[layers + 1] = jnp.zeros(cbuf.shape[1:], jnp.bfloat16)
+
+    def link(i, carry):
+        @pl.when(jnp.logical_not(jnp.logical_and(at_end, i == layers - 2)))
+        def _():
+            send_on(order(i))
+
         return carry
 
     lax.fori_loop(0, layers - 1, link, 0)
-    total = row_sum(z)
-    cbuf[layers + 1] = jnp.zeros(cbuf.shape[1:], jnp.bfloat16)
-
-    @pl.when(z > 0)
-    def _():
-        chain(z, z, me).wait_recv()
-
-    @pl.when(z + 1 < layers)
-    def _():
-        chain(z, layers, me).wait_recv()
-
-    from_low = cbuf[jnp.where(z > 0, z, layers + 1)].astype(jnp.float32)
-    from_high = cbuf[jnp.where(z + 1 < layers, layers, layers + 1)].astype(jnp.float32)
-    acc = total + from_low + from_high
-    ffn = acc.astype(jnp.bfloat16).astype(jnp.float32)
-    out[...] = (mid[...].astype(jnp.float32) + ffn).astype(jnp.bfloat16)
+    for h in range(PIECES):
+        total = row_sum(z, h)
+
+        @pl.when(z > 0)
+        def _():
+            chain(z, z, me, h).wait_recv()
+
+        @pl.when(z + 1 < layers)
+        def _():
+            chain(z, layers, me, h).wait_recv()
+
+        from_low = cbuf[jnp.where(z > 0, z, layers + 1), :, strips[h]]
+        from_high = cbuf[jnp.where(z + 1 < layers, layers, layers + 1), :, strips[h]]
+        total = total + from_low.astype(jnp.float32) + from_high.astype(jnp.float32)
+        ffn = total.astype(jnp.bfloat16).astype(jnp.float32)
+        out[:, strips[h]] = (mid[:, strips[h]].astype(jnp.float32) + ffn).astype(jnp.bfloat16)
 
     @pl.when(x == 0)
     def _():
@@ -709,20 +820,21 @@
 
     def drain(a, carry):
         for b in range(2):
-            for copy in across_x(a, b):
-                copy.wait_send()
+            sent_across(a, b)
             forward(a * 2 + b).wait_send()
             swap_sums(a * 2 + b).wait_send()
             tail(a * 2 + b).wait_send()
         for copy in in_plane(a) + corner(a):
             copy.wait_send()
         spread(a).wait_send()
-        across(a).wait_send()
+        for h in range(PIECES):
+            across(a, h).wait_send()
 
         @pl.when(a != z)
         def _():
             answer(a).wait_send()
-            chain(a, a, me).wait_send()
+            for h in range(PIECES):
+                chain(a, a, me, h).wait_send()
 
         @pl.when(jnp.logical_and(a <= z, z + 1 < layers))
         def _():
@@ -734,11 +846,11 @@
 
         @pl.when(a > 0)
         def _():
-            for copy in along_z(a) + weights(a, 0):
+            for copy in along_z(a):
                 copy.wait_send()
-
-        for copy in weights(a, 1):
-            copy.wait_send()
+            sent_weights(a, 0)
+
+        sent_weights(a, 1)
         return carry
 
     lax.fori_loop(0, layers, drain, 0)
@@ -777,17 +889,21 @@
     f32 = jnp.float32
     dma = pltpu.SemaphoreType.DMA
 
+    away = [pl.BlockSpec(memory_space=pl.ANY)]
+
     def room(*dims):
         return pltpu.VMEM(dims, bf)
 
     return pl.pallas_call(
         functools.partial(layer_kernel, n),
         out_shape=jax.ShapeDtypeStruct((half, model), bf),
-        in_specs=vm(3) + [pl.BlockSpec(memory_space=pltpu.SMEM)] + vm(9),
+        in_specs=vm(3)
+        + [pl.BlockSpec(memory_space=pltpu.SMEM)]
+        + vm(1) + away * 2 + vm(1) + away * 3 + vm(2),
         out_specs=vm(1)[0],
         scratch_shapes=[
             room(n * depth, wide), room(n * depth, wide), room(wide, n * depth),
-            room(half, model),
+            room(width, model), room(half, model), room(half, model),
             room(layers, rows, VD), room(n * rows, VD), room(n * rows, VD),
             room(layers, rows, VD),
             pltpu.VMEM((layers, 2 * rows, 4 * rows), f32),
@@ -796,13 +912,14 @@
             room(groups, rim, wide), room(groups + 1, rim, wide), room(rows, wide),
             room(groups, half, model), room(groups, half, model), room(groups, half, model),
             room(layers, half, model), room(layers, half, model), room(layers + 2, half, model),
-            dma((3, layers)), dma((3, layers)), dma((6, layers)), dma((6, layers)),
+            dma((8,)), dma((3, layers)), dma((3, layers)), dma((6, layers)), dma((6, layers)),
             dma((layers,)), dma((layers,)), dma((2,)),
-            dma((3, groups)), dma((3, groups)), dma((3, groups)), dma((3, groups)),
+            dma((6, groups)), dma((6, groups)), dma((6, groups)), dma((6, groups)),
             dma((layers,)), dma((layers,)), dma((layers,)), dma((layers,)), dma((layers,)),
             dma((groups,)), dma((groups,)), dma((groups,)), dma((groups,)),
-            dma((groups,)), dma((groups,)), dma((layers,)), dma((layers,)),
-            dma((layers,)), dma((layers + 1,)),
+            dma((groups,)), dma((groups,)),
+            dma((layers * PIECES,)), dma((layers * PIECES,)),
+            dma((layers * PIECES,)), dma(((layers + 1) * PIECES,)),
         ],
         compiler_params=pltpu.CompilerParams(
             collective_id=0, has_side_effects=True, vmem_limit_bytes=VMEM_LIMIT
@@ -821,9 +938,10 @@
         moves_rows = (
             n_tp == 2
             and n_sp % 4 == 0
+            and n_sp // 4 > 2
             and rest[2].shape[0] == n_sp // 4
             and up_weight.shape[1] % VD == 0
-            and up_weight.shape[1] // VD >= n_sp // 2
+            and up_weight.shape[1] // VD > n_sp // 2
             and queries.shape[0] % 32 == 0
             and up_weight.shape[0] % VD == 0
             and rest[8].shape[0] <= 16

time: 164 us -> 158 us (0.963); the launches traced: 162 us -> 158 us
  Pallas kernels: 160 us -> 156 us
    pallas_call x1, Pallas kernels: 160 us -> 156 us  [moving_rows(): pl.pallas_call(functools.partial(layer_kernel, n), out_shape=jax.ShapeDty...]
where the time goes in v3:
time: 158 us
  Pallas kernels  156 us (99%)
  local copies, waits for them, and re-layouts  1.77 us (1%)
    pallas_call x1, Pallas kernels, moving_rows(): pl.pallas_call(functools.partial(layer_kernel, n), out_shape=jax.ShapeDty...  156 us

profile of v3, /device:TPU:10, one launch (start us, length us, event | category | flops | bytes accessed | tf_op | source)
XLA Modules:
  0.0 158.0 jit_solution(17435480514335484680)
XLA Ops:
  0.0 156.2 %layer_rows.1 = bf16[96,2048]{1,0:T(8,128)(2,1)} custom-call(bf16[192,512]{1,0:T(8,128)(2,1)} %q.1, bf16[192,512]{1,0:T(8,128)(2,1)} %k.1, bf16[192,512]{1,0:T(8,128)(2,1)} %v.1, f32[4]{0:T(128)} %sw.1, f32[4,128]{1,0:T(4,128)} %bitcast.5, bf16[512,2048]{1,0:T(8,128)(2,1)} %ow.1, bf16[96,2048]{1,0:T(8,128)(2,1)} %res.1, f32[1,2048]{1,0:T(1,128)} %bitcast.4, ...), custom_call_target="tpu_custom_call" | custom-call | tf_op jit(solution)/shard_map/layer_rows/pallas_call | solution.py:897
  156.2 1.8 %copy.15 = bf16[96,2048]{1,0:T(8,128)(2,1)} copy(bf16[96,2048]{1,0:T(8,128)(2,1)} %layer_rows.1) | data formatting | bytes 786432

commit v4 on v3

--- a/solution.py
+++ b/solution.py
@@ -209,7 +209,7 @@
     n, q, k, v, sw, gain, ow, res, ngain, uw, gw, dw, cw, cb,
     out,
     wu, wg, wd, owb, resb, mid, qb, kb, vb, ob, sb, att, pbuf, prbuf,
-    buf, up, gate, tails, halo, hid, pb, pr, kept, rb, zb, cbuf,
+    buf, up, gate, tails, halo, hid, part_sum, pr, rb, zb, cbuf,
     lsem, zsend, zrecv, psend, precv, osend, orecv, tsem, wsend, wrecv, fsend, frecv,
     usend, dsend, lrecv, rsend, rrecv, csend, crecv, hsend, hrecv,
     xsend, xrecv, ysend, yrecv, ssend, srecv,
@@ -366,9 +366,8 @@
     qb[z] = q[:, cols(z)]
     for copy in in_plane(0):
         copy.start()
-    for a in range(1, layers):
-        send_weights(a, 0)
     send_weights(0, 1)
+    send_weights(2, 0)
 
     @pl.when(jnp.logical_not(full))
     def _():
@@ -395,6 +394,8 @@
 
     lax.fori_loop(1, layers, stage, 0)
     corner_stage(layers - 1)
+    send_weights(1, 0)
+    send_weights(3, 0)
     send_across(0, 0)
 
     def settle(a, carry):
@@ -520,43 +521,50 @@
     rim = tails.shape[1]
     taps = cw.shape[0]
 
-    def line_up(zz):
-        slot = zz * 2 + y
+    strip = out.shape[1] // PIECES
+    strips = [slice(h * strip, (h + 1) * strip) for h in range(PIECES)]
+
+    def ahead_of(slot, h):
+        return buf.at[slot, mine, strips[h]]
+
+    def line_up(zz, h):
+        ref = ahead_of(zz * 2 + y, h)
+        s = zz * PIECES + h
         dest = here.chip(jnp.minimum(z + 1, layers - 1), y, x)
-        return to_sp(buf.at[slot, mine], buf.at[slot, mine], usend.at[zz], lrecv.at[zz], dest)
-
-    def line_down(zz):
-        slot = zz * 2 + y
+        return to_sp(ref, ref, usend.at[s], lrecv.at[s], dest)
+
+    def line_down(zz, h):
+        ref = ahead_of(zz * 2 + y, h)
+        s = zz * PIECES + h
         dest = here.chip(jnp.maximum(z - 1, 0), y, x)
-        return to_sp(buf.at[slot, mine], buf.at[slot, mine], dsend.at[zz], lrecv.at[zz], dest)
-
-    def spread(zz):
-        slot = zz * 2 + y
-        return to_sp(
-            buf.at[slot, mine], buf.at[slot, mine], rsend.at[zz], rrecv.at[zz], here.yn
-        )
-
-    def spread_in(zz):
-        slot = zz * 2 + 1 - y
-        return to_sp(
-            buf.at[slot, mine], buf.at[slot, mine], rsend.at[zz], rrecv.at[zz], here.yn
-        )
-
-    def forward(slot):
-        return to_tp(
-            buf.at[slot, mine], buf.at[slot, mine], csend.at[slot], crecv.at[slot], 1 - t
-        )
-
-    def arrived(slot):
-        return to_tp(
-            buf.at[slot, theirs], buf.at[slot, theirs], csend.at[slot], crecv.at[slot], 1 - t
-        )
+        return to_sp(ref, ref, dsend.at[s], lrecv.at[s], dest)
+
+    def spread(zz, h):
+        ref = ahead_of(zz * 2 + y, h)
+        s = zz * PIECES + h
+        return to_sp(ref, ref, rsend.at[s], rrecv.at[s], here.yn)
+
+    def spread_in(zz, h):
+        ref = ahead_of(zz * 2 + 1 - y, h)
+        s = zz * PIECES + h
+        return to_sp(ref, ref, rsend.at[s], rrecv.at[s], here.yn)
+
+    def forward(slot, h):
+        ref = ahead_of(slot, h)
+        s = slot * PIECES + h
+        return to_tp(ref, ref, csend.at[s], crecv.at[s], 1 - t)
+
+    def arrived(slot, h):
+        ref = buf.at[slot, theirs, strips[h]]
+        s = slot * PIECES + h
+        return to_tp(ref, ref, csend.at[s], crecv.at[s], 1 - t)
 
     def tail(j):
         return to_sp(tails.at[j], halo.at[j + 1], hsend.at[j], hrecv.at[j], here.xn)
 
     def compute(j):
-        arrived(j).wait_recv()
+        for h in range(PIECES):
+            arrived(j, h).wait_recv()
         rows_in = buf[j]
         up_v = jnp.dot(rows_in, wu[...], preferred_element_type=jnp.float32).astype(jnp.bfloat16)
         up[span(j, rows), :] = up_v
@@ -568,14 +576,17 @@
 
     @pl.when(z + 1 < layers)
     def _():
-        line_up(z).start()
+        for h in range(PIECES):
+            line_up(z, h).start()
 
     @pl.when(z > 0)
     def _():
-        line_down(z).start()
-
-    spread(z).start()
-    forward(home).start()
+        for h in range(PIECES):
+            line_down(z, h).start()
+
+    for h in range(PIECES):
+        spread(z, h).start()
+        forward(home, h).start()
 
     def late(a, carry):
         pass_on(a, 1)
@@ -585,28 +596,29 @@
 
     def line_step(d):
         low, high = z - d, z + d
-
-        @pl.when(low >= 0)
-        def _():
-            line_up(low).wait_recv()
-
-            @pl.when(z + 1 < layers)
+        for h in range(PIECES):
+
+            @pl.when(low >= 0)
             def _():
-                line_up(low).start()
-
-            spread(low).start()
-            forward(low * 2 + y).start()
-
-        @pl.when(high < layers)
-        def _():
-            line_down(high).wait_recv()
-
-            @pl.when(z > 0)
+                line_up(low, h).wait_recv()
+
+                @pl.when(z + 1 < layers)
+                def _():
+                    line_up(low, h).start()
+
+                spread(low, h).start()
+                forward(low * 2 + y, h).start()
+
+            @pl.when(high < layers)
             def _():
-                line_down(high).start()
-
-            spread(high).start()
-            forward(high * 2 + y).start()
+                line_down(high, h).wait_recv()
+
+                @pl.when(z > 0)
+                def _():
+                    line_down(high, h).start()
+
+                spread(high, h).start()
+                forward(high * 2 + y, h).start()
 
     line_step(1)
 
@@ -636,14 +648,16 @@
         @pl.when(has_low)
         def _():
             compute(low * 2 + y)
-            spread_in(low).wait_recv()
-            forward(low * 2 + 1 - y).start()
+            for h in range(PIECES):
+                spread_in(low, h).wait_recv()
+                forward(low * 2 + 1 - y, h).start()
 
         @pl.when(has_high)
         def _():
             compute(high * 2 + y)
-            spread_in(high).wait_recv()
-            forward(high * 2 + 1 - y).start()
+            for h in range(PIECES):
+                spread_in(high, h).wait_recv()
+                forward(high * 2 + 1 - y, h).start()
 
         @pl.when(has_low)
         def _():
@@ -674,15 +688,14 @@
         return jnp.where(i >= layers - 1, z, pick)
 
     def swap_sums(slot):
-        return to_tp(pb.at[slot], pr.at[slot], xsend.at[slot], xrecv.at[slot], 1 - t)
-
-    strip = out.shape[1] // PIECES
-    strips = [slice(h * strip, (h + 1) * strip) for h in range(PIECES)]
+        return to_tp(
+            part_sum.at[slot, theirs], pr.at[slot], xsend.at[slot], xrecv.at[slot], 1 - t
+        )
 
     def across(zz, h):
         s = zz * PIECES + h
         return to_sp(
-            kept.at[zz * 2 + 1 - y, :, strips[h]], rb.at[zz, :, strips[h]],
+            part_sum.at[zz * 2 + 1 - y, mine, strips[h]], rb.at[zz, :, strips[h]],
             ysend.at[s], yrecv.at[s], here.yn,
         )
 
@@ -719,20 +732,16 @@
     def product(i):
         slot = slot_of(i)
         hidden(slot)
-        pb[slot] = jnp.dot(hid[theirs, :], wd[...], preferred_element_type=jnp.float32).astype(
-            jnp.bfloat16
-        )
+        part_sum[slot] = jnp.dot(
+            hid[...], wd[...], preferred_element_type=jnp.float32
+        ).astype(jnp.bfloat16)
         swap_sums(slot).start()
-        kept[slot] = jnp.dot(hid[mine, :], wd[...], preferred_element_type=jnp.float32).astype(
-            jnp.bfloat16
-        )
 
     def combine(i):
         slot = slot_of(i)
         swap_sums(slot).wait_recv()
-        kept[slot] = (kept[slot].astype(jnp.float32) + pr[slot].astype(jnp.float32)).astype(
-            jnp.bfloat16
-        )
+        kept = part_sum[slot, mine, :].astype(jnp.float32)
+        part_sum[slot, mine, :] = (kept + pr[slot].astype(jnp.float32)).astype(jnp.bfloat16)
 
         @pl.when(i < layers)
         def _():
@@ -741,9 +750,8 @@
 
     def row_sum(zz, h):
         across(zz, h).wait_recv()
-        return kept[zz * 2 + y, :, strips[h]].astype(jnp.float32) + rb[zz, :, strips[h]].astype(
-            jnp.float32
-        )
+        kept = part_sum[zz * 2 + y, mine, strips[h]].astype(jnp.float32)
+        return kept + rb[zz, :, strips[h]].astype(jnp.float32)
 
     def send_on(zz):
         rising = zz > z
@@ -821,12 +829,14 @@
     def drain(a, carry):
         for b in range(2):
             sent_across(a, b)
-            forward(a * 2 + b).wait_send()
+            for h in range(PIECES):
+                forward(a * 2 + b, h).wait_send()
             swap_sums(a * 2 + b).wait_send()
             tail(a * 2 + b).wait_send()
         for copy in in_plane(a) + corner(a):
             copy.wait_send()
-        spread(a).wait_send()
+        for h in range(PIECES):
+            spread(a, h).wait_send()
         for h in range(PIECES):
             across(a, h).wait_send()
 
@@ -838,11 +848,13 @@
 
         @pl.when(jnp.logical_and(a <= z, z + 1 < layers))
         def _():
-            line_up(a).wait_send()
+            for h in range(PIECES):
+                line_up(a, h).wait_send()
 
         @pl.when(jnp.logical_and(a >= z, z > 0))
         def _():
-            line_down(a).wait_send()
+            for h in range(PIECES):
+                line_down(a, h).wait_send()
 
         @pl.when(a > 0)
         def _():
@@ -910,13 +922,14 @@
             room(rows, width), room(half, model), room(half, model),
             room(groups, rows, model), room(groups * rows, wide), room(groups * rows, wide),
             room(groups, rim, wide), room(groups + 1, rim, wide), room(rows, wide),
-            room(groups, half, model), room(groups, half, model), room(groups, half, model),
+            room(groups, rows, model), room(groups, half, model),
             room(layers, half, model), room(layers, half, model), room(layers + 2, half, model),
             dma((8,)), dma((3, layers)), dma((3, layers)), dma((6, layers)), dma((6, layers)),
             dma((layers,)), dma((layers,)), dma((2,)),
             dma((6, groups)), dma((6, groups)), dma((6, groups)), dma((6, groups)),
-            dma((layers,)), dma((layers,)), dma((layers,)), dma((layers,)), dma((layers,)),
-            dma((groups,)), dma((groups,)), dma((groups,)), dma((groups,)),
+            dma((layers * PIECES,)), dma((layers * PIECES,)), dma((layers * PIECES,)),
+            dma((layers * PIECES,)), dma((layers * PIECES,)),
+            dma((groups * PIECES,)), dma((groups * PIECES,)), dma((groups,)), dma((groups,)),
             dma((groups,)), dma((groups,)),
             dma((layers * PIECES,)), dma((layers * PIECES,)),
             dma((layers * PIECES,)), dma(((layers + 1) * PIECES,)),

time: 158 us -> 156 us (0.987)
  Pallas kernels: 156 us -> 154 us
    pallas_call x1, Pallas kernels: 156 us -> 154 us  [moving_rows(): pl.pallas_call(functools.partial(layer_kernel, n), out_shape=jax.ShapeDty...]
where the time goes in v4:
time: 156 us; the launch traced here: 155 us
  Pallas kernels  154 us (99%)
  local copies, waits for them, and re-layouts  1.77 us (1%)
    pallas_call x1, Pallas kernels, moving_rows(): pl.pallas_call(functools.partial(layer_kernel, n), out_shape=jax.ShapeDty...  154 us

profile of v4, /device:TPU:10, one launch (start us, length us, event | category | flops | bytes accessed | tf_op | source)
XLA Modules:
  0.0 155.3 jit_solution(1106345259514545810)
XLA Ops:
  0.0 153.6 %layer_rows.1 = bf16[96,2048]{1,0:T(8,128)(2,1)} custom-call(bf16[192,512]{1,0:T(8,128)(2,1)} %q.1, bf16[192,512]{1,0:T(8,128)(2,1)} %k.1, bf16[192,512]{1,0:T(8,128)(2,1)} %v.1, f32[4]{0:T(128)} %sw.1, f32[4,128]{1,0:T(4,128)} %bitcast.5, bf16[512,2048]{1,0:T(8,128)(2,1)} %ow.1, bf16[96,2048]{1,0:T(8,128)(2,1)} %res.1, f32[1,2048]{1,0:T(1,128)} %bitcast.4, ...), custom_call_target="tpu_custom_call" | custom-call | tf_op jit(solution)/shard_map/layer_rows/pallas_call | solution.py:909
  153.6 1.8 %copy.15 = bf16[96,2048]{1,0:T(8,128)(2,1)} copy(bf16[96,2048]{1,0:T(8,128)(2,1)} %layer_rows.1) | data formatting | bytes 786432

commit v5 on v4

--- a/solution.py
+++ b/solution.py
@@ -142,18 +142,20 @@
     return (mid.astype(jnp.float32) + ffn_out.astype(jnp.float32)).astype(jnp.bfloat16)
 
 
-def greet(n, me, t):
+def greet(here):
     barrier = pltpu.get_barrier_semaphore()
+    groups = here.n // 2
 
     def signal(k, carry):
-        pl.semaphore_signal(
-            barrier, inc=1, device_id={"sp": lax.rem(me + k, n)}, device_id_type=MESH
-        )
-        return carry
-
-    lax.fori_loop(1, n, signal, 0)
-    pl.semaphore_signal(barrier, inc=1, device_id={"tp": 1 - t}, device_id_type=MESH)
-    pl.semaphore_wait(barrier, n)
+        j = lax.rem(here.z * 2 + here.y + k, groups)
+        dest = here.chip(j // 2, lax.rem(j, 2), here.x)
+        pl.semaphore_signal(barrier, inc=1, device_id={"sp": dest}, device_id_type=MESH)
+        return carry
+
+    lax.fori_loop(1, groups, signal, 0)
+    pl.semaphore_signal(barrier, inc=1, device_id={"sp": here.xn}, device_id_type=MESH)
+    pl.semaphore_signal(barrier, inc=1, device_id={"tp": 1 - here.t}, device_id_type=MESH)
+    pl.semaphore_wait(barrier, groups + 1)
 
 
 def to_sp(src, dst, send, recv, dest):
@@ -356,7 +358,7 @@
     for copy in side_copies():
         copy.start()
 
-    greet(n, me, t)
+    greet(here)
 
     for a in range(1, layers):
         for copy in along_z(a):

time: 156 us -> 155 us (level)
  Pallas kernels: 154 us -> 151 us
    pallas_call x1, Pallas kernels: 154 us -> 151 us  [moving_rows(): pl.pallas_call(functools.partial(layer_kernel, n), out_shape=jax.ShapeDty...]
where the time goes in v5:
time: 155 us; the launch traced here: 153 us
  Pallas kernels  151 us (97%)
  local copies, waits for them, and re-layouts  1.77 us (1%)
    pallas_call x1, Pallas kernels, moving_rows(): pl.pallas_call(functools.partial(layer_kernel, n), out_shape=jax.ShapeDty...  151 us

profile of v5, /device:TPU:10, one launch (start us, length us, event | category | flops | bytes accessed | tf_op | source)
XLA Modules:
  0.0 152.9 jit_solution(9753437477054704409)
XLA Ops:
  0.0 151.1 %layer_rows.1 = bf16[96,2048]{1,0:T(8,128)(2,1)} custom-call(bf16[192,512]{1,0:T(8,128)(2,1)} %q.1, bf16[192,512]{1,0:T(8,128)(2,1)} %k.1, bf16[192,512]{1,0:T(8,128)(2,1)} %v.1, f32[4]{0:T(128)} %sw.1, f32[4,128]{1,0:T(4,128)} %bitcast.5, bf16[512,2048]{1,0:T(8,128)(2,1)} %ow.1, bf16[96,2048]{1,0:T(8,128)(2,1)} %res.1, f32[1,2048]{1,0:T(1,128)} %bitcast.4, ...), custom_call_target="tpu_custom_call" | custom-call | tf_op jit(solution)/shard_map/layer_rows/pallas_call | solution.py:911
  151.1 1.8 %copy.15 = bf16[96,2048]{1,0:T(8,128)(2,1)} copy(bf16[96,2048]{1,0:T(8,128)(2,1)} %layer_rows.1) | data formatting | bytes 786432
